TPU v7x, 512 devices: a whole 4x4x16 slice. The times are simulated.
512 devices in a mesh: dp: 4 (over x), kv: 64 (over z, y), tp: 2 (over core).
Axes of the slice: x: 4, y: 4, z: 16, core: 2. Of those that a mesh axis runs over, the one named last changes fastest.
Arguments:
- tokens: bfloat16 [16, 24, 2048], P('dp'), may hold values from -6 to 6
- norm_gain: bfloat16 [2048], replicated, may hold values from 0.099609375 to 1.8984375
- w_query: bfloat16 [2048, 1024], P('kv', 'tp'), may hold values from -0.125 to 0.125
- w_key: bfloat16 [2048, 1024], P('kv', 'tp'), may hold values from -0.03125 to 0.03125
- w_value: bfloat16 [2048, 1024], P('kv', 'tp'), may hold values from -0.03125 to 0.03125
- w_forget: bfloat16 [2048, 16], P('kv', 'tp'), may hold values from -0.125 to 0.125
- forget_bias: float32 [16], P('tp'), may hold values from 0 to 4
- head_gain: bfloat16 [1024], P('tp'), may hold values from 0.099609375 to 1.8984375
- w_out: bfloat16 [1024, 2048], P('tp', 'kv'), may hold values from -0.1875 to 0.1875
- cache_keys: bfloat16 [16, 16384, 1024], P('dp', 'kv', 'tp'), may hold values from -480 to 480
- cache_values: bfloat16 [16, 16384, 1024], P('dp', 'kv', 'tp'), may hold values from -1.5 to 1.5
- cache_gates: float32 [16, 16, 16384], P('dp', 'tp', 'kv'), may hold values from -2048 to 0, as said below
- lengths: int32 [16], P('dp'), may hold values from 8192 to 16335
- accepted: int32 [16], P('dp'), may hold values from 0 to 23
- parents: int32 [16, 24], P('dp'), may hold values from -1 to 22, as said below
Outputs:
- mixed: float32 [16, 24, 2048], P('dp', None, ('kv', 'tp'))
- keys_out: bfloat16 [16, 16384, 1024], P('dp', 'kv', 'tp')
- values_out: bfloat16 [16, 16384, 1024], P('dp', 'kv', 'tp')
- gates_out: float32 [16, 16, 16384], P('dp', 'tp', 'kv')
Inputs may be any that keep to these rules, and one draw needn't show every extreme that they name: parents[b, 0] = -1 and 0 <= parents[b, j] < j for every later proposal j. `cache_gates`: nonincreasing along the positions of each sequence and head.
All inputs are finite; a program needn't handle non-finite values.
Results may differ from a plain program's by a relative error of at most 0.008.
Values may be sent and summed in bfloat16 or wider, within the bound.
No kernel may reach another device: no remote copies, remote signals or barrier semaphores. Data moves between devices by JAX's collectives and lax.ppermute only.
A program may use at most 64 MiB of HBM per device.

v0:
```python
import jax
import jax.numpy as jnp
from jax import lax
from jax.sharding import Mesh
from jax.sharding import PartitionSpec as P

KV = ("kv_0", "kv_1")
KV_TP = ("kv_0", "kv_1", "tp")


NEG_LARGE = -1e30
EPSILON = 1e-06


def in_one_piece(arrays, axis, dim, along):
    widths = [a.shape[along] for a in arrays]
    both = jnp.concatenate(arrays, axis=along)
    whole = lax.all_gather(both, axis, axis=dim, tiled=True)
    return tuple(jnp.split(whole, [sum(widths[:k]) for k in range(1, len(widths))], axis=along))


def one_axis_at_a_time(array, axes):
    for axis in axes:
        array = lax.psum(array, axis)
    return array


def collected_together(array, axis):
    leaves = jax.tree.leaves(array)
    sequence = sorted(range(len(leaves)), key=lambda k: -leaves[k].size)
    width = (1, *leaves[sequence[0]].shape)[-1]
    lines = [
        jnp.pad(leaves[k].reshape(-1), (0, -leaves[k].size % width)).reshape(-1, width)
        for k in sequence
    ]
    both, at, found = (lax.all_gather(jnp.concatenate(lines), axis), 0, {})
    for k, line in zip(sequence, lines):
        piece = both[:, at : at + len(line)].reshape(len(both), -1)
        found[k] = piece[:, : leaves[k].size].reshape(-1, *leaves[k].shape)
        at += len(line)
    numbers = iter(range(len(leaves)))
    return jax.tree.map(lambda _: found[next(numbers)], array)


def merged_by_axis(array, axes, combine):
    for axis in axes:
        pieces = collected_together(array, axis)
        array = jax.tree.map(lambda part: part[0], pieces)
        for k in range(1, lax.axis_size(axis)):
            array = combine(array, jax.tree.map(lambda part: part[k], pieces))
    return array


def in_blocks(array, dim, peers):
    before, after = (array.shape[:dim], array.shape[dim + 1 :])
    return jnp.moveaxis(array.reshape(*before, peers, -1, *after), dim, 0)


def sent_and_summed(array, axis, dim):
    pieces = in_blocks(array, dim, lax.axis_size(axis))
    arrived = lax.all_to_all(pieces, axis, split_axis=0, concat_axis=0, tiled=True)
    return arrived.sum(axis=0)


def ancestry(parents):
    prop_count = parents.shape[1]
    indices = jnp.arange(prop_count, dtype=jnp.int32)
    linked = (parents[:, :, None] == indices[None, None, :]).astype(jnp.float32)
    linked = linked + (indices[:, None] == indices[None, :]).astype(jnp.float32)[None]
    for repeat in range(prop_count.bit_length()):
        linked = jnp.minimum(jnp.einsum("bij,bjk->bik", linked, linked), 1.0)
    return linked


def merge_pair(first_part, second_part):
    highest = jnp.maximum(first_part[0], second_part[0])
    scale_first = jnp.exp(first_part[0] - highest)
    scale_second = jnp.exp(second_part[0] - highest)
    seq_count, prop_count, head_count = highest.shape
    outer_first = (
        first_part[2].reshape(seq_count, prop_count, head_count, -1) * scale_first[..., None]
    )
    outer_second = (
        second_part[2].reshape(seq_count, prop_count, head_count, -1) * scale_second[..., None]
    )
    joined = (outer_first + outer_second).reshape(seq_count, prop_count, -1)
    return (highest, first_part[1] * scale_first + second_part[1] * scale_second, joined)


def local(
    tokens,
    norm_gain,
    w_query,
    w_key,
    w_value,
    w_forget,
    forget_bias,
    head_gain,
    w_out,
    cache_keys,
    cache_values,
    cache_gates,
    lengths,
    accepted,
    parents,
):
    seq_count, prop_count, model_width = tokens.shape
    span_rows = cache_keys.shape[1]
    head_count = cache_gates.shape[1]
    head_size = cache_keys.shape[2] // head_count
    scale = head_size ** (-0.5)
    start_pos = lax.axis_index(KV) * span_rows
    positions = start_pos + jnp.arange(span_rows, dtype=jnp.int32)
    valid_len = lengths + accepted
    flat_rows = tokens.reshape(seq_count * prop_count, model_width).astype(jnp.float32)
    normed = (
        flat_rows
        * lax.rsqrt(jnp.mean(flat_rows * flat_rows, axis=1, keepdims=True) + EPSILON)
        * norm_gain.astype(jnp.float32)
    ).astype(jnp.bfloat16)
    picked = (positions[None, :] == (valid_len - 1)[:, None]).astype(jnp.float32)
    last_part = jnp.sum(cache_gates * picked[:, None, :], axis=2)
    pieces = in_one_piece((w_query, w_key, w_value, w_forget), KV, 0, 1)
    query, fresh_keys, fresh_values, gate_pre = tuple(
        (jnp.dot(normed, piece, preferred_element_type=jnp.float32) for piece in pieces)
    )
    last_gate = one_axis_at_a_time(last_part, KV)
    query = query.astype(jnp.bfloat16).reshape(seq_count, prop_count, head_count, head_size)
    fresh_keys = fresh_keys.astype(jnp.bfloat16).reshape(
        seq_count, prop_count, head_count, head_size
    )
    fresh_values = fresh_values.astype(jnp.bfloat16).reshape(
        seq_count, prop_count, head_count, head_size
    )
    log_gate = jax.nn.log_sigmoid(gate_pre + forget_bias).reshape(seq_count, prop_count, head_count)
    link = ancestry(parents)
    climb = jnp.einsum("bia,bah->bih", link, log_gate)
    stored_keys = cache_keys.reshape(seq_count, span_rows, head_count, head_size)
    stored_values = cache_values.reshape(seq_count, span_rows, head_count, head_size)
    scores = (
        jnp.einsum("bphd,bchd->bphc", query, stored_keys, preferred_element_type=jnp.float32)
        * scale
    )
    scores = scores + (last_gate[:, None, :] + climb)[..., None] - cache_gates[:, None]
    seen = (positions[None, :] < valid_len[:, None])[:, None, None, :]
    highest = jnp.max(jnp.where(seen, scores, NEG_LARGE), axis=3)
    weights = jnp.where(seen, jnp.exp(scores - highest[..., None]), 0.0)
    normalizer = jnp.sum(weights, axis=3)
    weighted = jnp.einsum(
        "bphc,bchd->bphd",
        weights.astype(jnp.bfloat16),
        stored_values,
        preferred_element_type=jnp.float32,
    )
    highest, normalizer, weighted = merged_by_axis(
        (highest, normalizer, weighted.reshape(seq_count, prop_count, head_count * head_size)),
        KV,
        merge_pair,
    )
    near_scores = (
        jnp.einsum("bphd,bahd->bpha", query, fresh_keys, preferred_element_type=jnp.float32) * scale
    )
    near_scores = near_scores + climb[..., None] - jnp.transpose(climb, (0, 2, 1))[:, None]
    linked = (link > 0.5)[:, :, None, :]
    near_high = jnp.max(jnp.where(linked, near_scores, NEG_LARGE), axis=3)
    overall = jnp.maximum(highest, near_high)
    carried = jnp.exp(highest - overall)
    near_weights = jnp.where(linked, jnp.exp(near_scores - overall[..., None]), 0.0)
    normalizer = normalizer * carried + jnp.sum(near_weights, axis=3)
    attended = weighted.reshape(seq_count, prop_count, head_count, head_size) * carried[..., None]
    attended = attended + jnp.einsum(
        "bpha,bahd->bphd",
        near_weights.astype(jnp.bfloat16),
        fresh_values,
        preferred_element_type=jnp.float32,
    )
    attended = attended / normalizer[..., None]
    gain_rows = head_gain.astype(jnp.float32).reshape(head_count, head_size)
    heads_out = (
        (
            attended
            * lax.rsqrt(jnp.mean(attended * attended, axis=3, keepdims=True) + EPSILON)
            * gain_rows
        )
        .astype(jnp.bfloat16)
        .reshape(seq_count * prop_count, head_count * head_size)
    )
    partial_sum = jnp.dot(heads_out, w_out, preferred_element_type=jnp.float32)
    summed = sent_and_summed(partial_sum, "tp", 1)
    mixed = summed.reshape(seq_count, prop_count, -1)
    offsets = positions[None, :, None] - valid_len[:, None, None]
    placed = offsets == jnp.arange(prop_count, dtype=jnp.int32)[None, None, :]
    landed = jnp.any(placed, axis=2)
    placed_low = placed.astype(jnp.bfloat16)
    written_keys = jnp.einsum(
        "bcj,bjx->bcx",
        placed_low,
        fresh_keys.reshape(seq_count, prop_count, -1),
        preferred_element_type=jnp.float32,
    ).astype(jnp.bfloat16)
    written_values = jnp.einsum(
        "bcj,bjx->bcx",
        placed_low,
        fresh_values.reshape(seq_count, prop_count, -1),
        preferred_element_type=jnp.float32,
    ).astype(jnp.bfloat16)
    keys_out = jnp.where(landed[..., None], written_keys, cache_keys)
    values_out = jnp.where(landed[..., None], written_values, cache_values)
    new_gates = last_gate[:, :, None] + jnp.transpose(climb, (0, 2, 1))
    written_gates = jnp.einsum("bcj,bhj->bhc", placed.astype(jnp.float32), new_gates)
    gates_out = jnp.where(landed[:, None, :], written_gates, cache_gates)
    return (mixed, keys_out, values_out, gates_out)


def solution(mesh):
    torus = Mesh(
        mesh.devices.reshape(mesh.shape["dp"], 16, 4, mesh.shape["tp"]),
        ("dp", "kv_0", "kv_1", "tp"),
    )
    return jax.shard_map(
        local,
        mesh=torus,
        in_specs=(
            P("dp", None, None),
            P(),
            P(KV, "tp"),
            P(KV, "tp"),
            P(KV, "tp"),
            P(KV, "tp"),
            P("tp"),
            P("tp"),
            P("tp", KV),
            P("dp", KV, "tp"),
            P("dp", KV, "tp"),
            P("dp", "tp", KV),
            P("dp"),
            P("dp"),
            P("dp", None),
        ),
        out_specs=(P("dp", None, KV_TP), P("dp", KV, "tp"), P("dp", KV, "tp"), P("dp", "tp", KV)),
        check_vma=False,
    )
```

profile of v0, /device:TPU:1, one launch (start us, length us, event | category | flops | bytes accessed | tf_op | source)
XLA Modules:
  0.0 345.5 jit_solution(17081064558434147819)
XLA Ops:
  8.2 1.4 pad_maximum_fusion
  11.6 2.3 copy.57
  15.3 30.6 %psum.14 = f32[4,8]{1,0:T(4,128)S(1)} all-reduce(f32[4,8]{1,0:T(4,128)S(1)} %multiply_reduce_fusion.2), channel_id=1, replica_groups=mesh['dp'=4,'kv_0'=16,'kv_1'=4,'tp'=2] {'kv_0'}, use_global_device_ids=true, to_apply=%region_2.0 | all-reduce | flops 32 | bytes 256 | tf_op jit(solution)/shard_map/psum | solution.py:24
  45.8 9.1 %psum.15 = f32[4,8]{1,0:T(4,128)S(1)} all-reduce(f32[4,8]{1,0:T(4,128)S(1)} %psum.14), channel_id=1, replica_groups=mesh['dp'=4,'kv_0'=16,'kv_1'=4,'tp'=2] {'kv_1'}, use_global_device_ids=true, to_apply=%region_3.0 | all-reduce | flops 32 | bytes 256 | tf_op jit(solution)/shard_map/psum | solution.py:24
  56.5 104.4 %all-gather.7.cloned.1.call-done = bf16[2048,1544]{1,0:T(8,128)(2,1)} async-done(((bf16[32,1544]{1,0:T(8,128)(2,1)}), bf16[2048,1544]{1,0:T(8,128)(2,1)}) %all-gather.7.cloned.1.call-update) | async-done | bytes 6324240 | tf_op jit(solution)/shard_map/all_gather | solution.py:18
  162.3 2.1 fusion.16
  165.3 1.6 select_reduce_fusion
  167.6 1.6 fusion.28
  170.6 1.5 reshape.1556
  174.6 1.5 reshape.1554
  180.0 1.4 maximum_bitcast_fusion
  183.8 2.1 fusion.19
  186.1 2.1 fusion.22
  189.8 1.6 select_reduce_fusion.1
  191.4 1.5 fusion.6
  192.9 1.5 fusion.7
  194.4 57.1 %all-gather.9.cloned.1.call-done = f32[16,100,512]{2,1,0:T(8,128)} async-done(((f32[1,100,512]{2,1,0:T(8,128)}), f32[16,100,512]{2,1,0:T(8,128)}) %all-gather.9.cloned.1.call-update) | async-done | bytes 3276816 | tf_op jit(solution)/shard_map/all_gather | solution.py:36
  280.8 2.0 mul.671
  282.7 1.7 mul.664
  284.5 1.8 mul.665
  286.3 1.7 mul.667
  288.0 1.8 mul.668
  289.8 1.7 mul.658
  291.5 1.8 mul.659
  293.3 1.7 mul.652
  295.1 1.8 mul.653
  297.8 2.0 mul.656
  300.7 1.8 mul.647
  302.5 3.8 %fusion.45 = f32[96,512]{1,0:T(8,128)S(1)} fusion(f32[96,512]{1,0:T(8,128)} %mul.731, f32[16,100,512]{2,1,0:T(8,128)S(1)} %copy-done.3, f32[96,512]{1,0:T(8,128)} %mul.728, f32[96,512]{1,0:T(8,128)} %mul.725, f32[96,512]{1,0:T(8,128)} %mul.722, f32[96,512]{1,0:T(8,128)} %mul.719, f32[96,512]{1,0:T(8,128)} %mul.716, f32[96,512]{1,0:T(8,128)} %mul.713, ...), kind=kLoop, calls=%fused_computation.66 | loop fusion | flops 2211840 | bytes 9240576 | tf_op jit(solution)/shard_map/add | solution.py:86
  306.4 11.0 %all-gather.3 = f32[4,100,512]{2,1,0:T(8,128)S(1)} all-gather(f32[1,100,512]{2,1,0:T(8,128)S(1)} %maximum_bitcast_fusion.1), channel_id=3, replica_groups=mesh['dp'=4,'kv_0'=16,'kv_1'=4,'tp'=2] {'kv_1'}, dimensions={0}, use_global_device_ids=true | all-gather | bytes 1024000 | tf_op jit(solution)/shard_map/all_gather | solution.py:36
  319.6 1.7 multiply_reduce_fusion.1
  321.9 16.0 %all_to_all.5 = f32[2,96,16]{1,2,0:T(8,128)S(1)} all-to-all(f32[2,96,16]{1,2,0:T(8,128)S(1)} %convolution_bitcast_fusion.2), channel_id=1, replica_groups=mesh['dp'=4,'kv_0'=16,'kv_1'=4,'tp'=2] {'tp'}, dimensions={0} | all-to-all | bytes 24576 | tf_op jit(solution)/shard_map/all_to_all | solution.py:61
  (201 shorter events, 54.9 us)
Async XLA Ops:
  7.2 314.6 %copy-start = (bf16[512,32]{0,1:T(8,128)(2,1)S(1)}, bf16[512,32]{0,1:T(8,128)(2,1)}, u32[]{:S(2)}) copy-start(bf16[512,32]{0,1:T(8,128)(2,1)} %param.23) | copy-start | bytes 98308
  7.2 49.1 %copy-start.4 = (bf16[4,24,2048]{2,1,0:T(8,128)(2,1)S(1)}, bf16[4,24,2048]{2,1,0:T(8,128)(2,1)}, u32[]{:S(2)}) copy-start(bf16[4,24,2048]{2,1,0:T(8,128)(2,1)} %param.15) | copy-start | bytes 1179652
  7.2 6.7 %copy-start.2 = (bf16[4,256,512]{2,1,0:T(8,128)(2,1)S(1)}, bf16[4,256,512]{2,1,0:T(8,128)(2,1)}, u32[]{:S(2)}) copy-start(bf16[4,256,512]{2,1,0:T(8,128)(2,1)} %param.25) | copy-start | bytes 3145732
  7.2 7.2 %copy-start.18 = (s32[4]{0:T(128)S(1)}, s32[4]{0:T(128)}, u32[]{:S(2)}) copy-start(s32[4]{0:T(128)} %param.28) | copy-start | bytes 52
  7.2 7.2 %copy-start.17 = (s32[4]{0:T(128)S(1)}, s32[4]{0:T(128)}, u32[]{:S(2)}) copy-start(s32[4]{0:T(128)} %param.27) | copy-start | bytes 52
  7.2 7.9 %copy-start.6 = (f32[4,8,256]{2,1,0:T(8,128)S(1)}, f32[4,8,256]{2,1,0:T(8,128)}, u32[]{:S(2)}) copy-start(f32[4,8,256]{2,1,0:T(8,128)} %param.26) | copy-start | bytes 98308
  7.2 47.6 %copy-start.19 = (s32[4,24]{1,0:T(4,128)S(1)}, s32[4,24]{1,0:T(4,128)}, u32[]{:S(2)}) copy-start(s32[4,24]{1,0:T(4,128)} %param.29) | copy-start | bytes 1156
  7.2 153.6 %copy-start.16 = (f32[8]{0:T(128)S(1)}, f32[8]{0:T(128)}, u32[]{:S(2)}) copy-start(f32[8]{0:T(128)} %param.21) | copy-start | bytes 100
  7.3 153.6 %all-gather.7.cloned.1.call-start = ((), (), s32[]{:S(2)}) async-start(), calls=%async_computation.1 | async-start | bytes 6922240 | tf_op jit(solution)/shard_map/all_gather | solution.py:18
  9.6 241.9 %all-gather.9.cloned.1.call-start = ((), (), s32[]{:S(2)}) async-start(), calls=%async_computation.2 | async-start | bytes 3620864 | tf_op jit(solution)/shard_map/all_gather | solution.py:36
  14.5 147.8 %copy-start.15 = (s32[256]{0:T(256)}, s32[256]{0:T(256)S(1)}, u32[]{:S(2)}) copy-start(s32[256]{0:T(256)S(1)} %iota_add_fusion) | copy-start | bytes 3076
  14.5 0.7 copy-start.14
  54.9 110.4 %copy-start.9 = (f32[4,8]{1,0:T(4,128)}, f32[4,8]{1,0:T(4,128)S(1)}, u32[]{:S(2)}) copy-start(f32[4,8]{1,0:T(4,128)S(1)} %psum.15) | copy-start | bytes 388
  181.5 7.6 %copy-start.8 = (f32[4,24,8]{1,2,0:T(8,128)S(1)}, f32[4,24,8]{1,2,0:T(8,128)}, u32[]{:S(2)}) copy-start(f32[4,24,8]{1,2,0:T(8,128)} %get-tuple-element.142) | copy-start | bytes 9220
  181.5 7.6 %copy-start.10 = (f32[4,8]{1,0:T(4,128)S(1)}, f32[4,8]{1,0:T(4,128)}, u32[]{:S(2)}) copy-start(f32[4,8]{1,0:T(4,128)} %copy-done.9) | copy-start | bytes 388
  183.8 7.6 %copy-start.1 = (bf16[4,256,512]{2,1,0:T(8,128)(2,1)S(1)}, bf16[4,256,512]{2,1,0:T(8,128)(2,1)}, u32[]{:S(2)}) copy-start(bf16[4,256,512]{2,1,0:T(8,128)(2,1)} %param.24) | copy-start | bytes 3145732
  280.8 21.7 %copy-start.3 = (f32[16,100,512]{2,1,0:T(8,128)S(1)}, f32[16,100,512]{2,1,0:T(8,128)}, u32[]{:S(2)}) copy-start(f32[16,100,512]{2,1,0:T(8,128)} %all-gather.9.cloned.1.call-done) | copy-start | bytes 9830404
  302.5 3.8 %copy-start.11 = (f32[2,512]{1,0:T(2,128)S(1)}, f32[2,512]{1,0:T(2,128)}, u32[]{:S(2)}) copy-start(f32[2,512]{1,0:T(2,128)} %reshape.1561) | copy-start | bytes 12292
  302.5 3.8 %copy-start.12 = (f32[2,512]{1,0:T(2,128)S(1)}, f32[2,512]{1,0:T(2,128)}, u32[]{:S(2)}) copy-start(f32[2,512]{1,0:T(2,128)} %reshape.1559) | copy-start | bytes 12292
  306.3 13.1 %copy-start.13 = (f32[4,24,8]{1,2,0:T(8,128)S(1)}, f32[4,24,8]{1,2,0:T(8,128)}, u32[]{:S(2)}) copy-start(f32[4,24,8]{1,2,0:T(8,128)} %get-tuple-element.147) | copy-start | bytes 9220
  306.4 13.1 %copy-start.5 = (f32[4,24,8,24]{1,3,2,0:T(8,128)S(1)}, f32[4,24,8,24]{1,3,2,0:T(8,128)}, u32[]{:S(2)}) copy-start(f32[4,24,8,24]{1,3,2,0:T(8,128)} %get-tuple-element.148) | copy-start | bytes 221188
  306.4 13.2 %copy-start.7 = (bf16[4,24,8,64]{3,2,1,0:T(8,128)(2,1)S(1)}, bf16[4,24,8,64]{3,2,1,0:T(8,128)(2,1)}, u32[]{:S(2)}) copy-start(bf16[4,24,8,64]{3,2,1,0:T(8,128)(2,1)} %reshape.1564) | copy-start | bytes 294916
Sparse Core Ops, SparseCore 0:
  11.6 149.2 all-gather.6
  181.6 69.8 all-gather.8
where the time goes:
time: 347 us; the launch traced here: 345 us
  waiting for transfers between devices  162 us (47%)
  local copies, waits for them, and re-layouts  68.7 us (20%)
  blocking collectives  66.7 us (19%)
  matrix products  19.6 us (6%)
  between operations  14.9 us (4%)
  other arithmetic  13.9 us (4%)
    all_gather x1, waiting for transfers between devices, in_one_piece(): whole = lax.all_gather(both, axis, axis=dim, tiled=True)  104 us
    all_gather x1, waiting for transfers between devices, collected_together(): both, at, found = (lax.all_gather(jnp.concatenate(lines), axis), 0, {})  57.1 us
    psum x2, blocking collectives, one_axis_at_a_time(): array = lax.psum(array, axis)  39.6 us
    mul x30, local copies, waits for them, and re-layouts, merge_pair(): second_part[2].reshape(seq_count, prop_count, head_count, -1)  26 us
    mul x30, local copies, waits for them, and re-layouts, merge_pair(): first_part[2].reshape(seq_count, prop_count, head_count, -1)  19.1 us
    all_to_all x1, blocking collectives, sent_and_summed(): lax.all_to_all(pieces, axis, split_axis=0, concat_axis=0, tiled=True)  16 us
    all_gather x1, blocking collectives, collected_together(): both, at, found = (lax.all_gather(jnp.concatenate(lines), axis), 0, {})  11 us
    dot_general x4, matrix products, local(): jnp.dot(normed, piece, preferred_element_type=jnp.float32)  7.6 us
  transfers between devices with their start and end apart: 2, of which 2 were waited for; matrix products, arithmetic and copies ran while one was open for 6% of the time, Pallas kernels for 0%

commit v1 on v0

v1 whole, which is shorter than its diff:
```python
import jax
import jax.numpy as jnp
from jax import lax
from jax.experimental import pallas as pl
from jax.experimental.pallas import tpu as pltpu
from jax.sharding import Mesh
from jax.sharding import PartitionSpec as P

KV = ("kv_0", "kv_1")
KV_TP = ("kv_0", "kv_1", "tp")

NEG_LARGE = -1e30
EPSILON = 1e-06
F32 = jnp.float32
BF16 = jnp.bfloat16

GROUP = 6
SLOTS = 8
NT = (((1,), (1,)), ((), ()))
INTERPRET = False


def iota(shape, dim):
    return lax.broadcasted_iota(jnp.int32, shape, dim)


def three_parts(x):
    high = x.astype(BF16).astype(F32)
    rest = x - high
    middle = rest.astype(BF16).astype(F32)
    return high, middle, rest - middle


def pack_kernel(wq_ref, wk_ref, wv_ref, wf_ref, out_ref):
    rows = wq_ref.shape[0]
    stacked = jnp.concatenate(
        [wq_ref[...].astype(F32), wk_ref[...].astype(F32), wv_ref[...].astype(F32), jnp.zeros((rows, wq_ref.shape[1]), F32)],
        axis=0,
    )
    turned = stacked.T.reshape(out_ref.shape)
    forget = jnp.concatenate([jnp.zeros((8, 3 * rows), F32), wf_ref[...].astype(F32)], axis=1)
    lane = iota((1, 8, 128), 2)
    out_ref[...] = jnp.where(lane >= 3 * rows, forget[None], turned).astype(BF16)


def project_kernel(x_ref, tok_ref, gain_ref, bias_ref, par_ref, piece_ref, climb_ref, link_ref, wt_ref, nrm_ref):
    x = x_ref[...].astype(F32).reshape(16, 4, 8, 128)
    block = iota((128, 128), 1) // 32
    for t in range(4):
        row = None
        for n in range(4):
            moved = x[:, n].reshape(128, 128)
            if n != t:
                moved = pltpu.roll(moved, ((n - t) * 32) % 128, 1)
            row = moved if row is None else jnp.where(block == n, moved, row)
        row = row.reshape(16, 8, 128)
        for m in range(16):
            wt_ref[t * 8 : (t + 1) * 8, m * 128 : (m + 1) * 128] = row[m]
    nrm_ref[...] = jnp.zeros(nrm_ref.shape, F32)
    gain = gain_ref[...].astype(F32)
    for b in range(4):
        tok = tok_ref[b].astype(F32)
        normed = tok * lax.rsqrt(jnp.mean(tok * tok, axis=1, keepdims=True) + EPSILON) * gain
        for g in range(4):
            at = b * 32 + g * SLOTS
            nrm_ref[at : at + GROUP, :] = normed[g * GROUP : (g + 1) * GROUP]
    out = lax.dot_general(
        wt_ref[...].astype(BF16), nrm_ref[...].astype(BF16), NT, preferred_element_type=F32
    )
    piece = out[:24].reshape(3, 8, 128).astype(BF16)
    piece_ref[...] = jnp.broadcast_to(piece[None], piece_ref.shape)
    pre = out[24:] + bias_ref[...]
    log_gate = jnp.minimum(pre, 0.0) - jnp.log1p(jnp.exp(-jnp.abs(pre)))
    child = iota((128, 128), 0)
    linked = ((par_ref[...] == child) | (child == iota((128, 128), 1))).astype(F32)
    for repeat in range(5):
        low = linked.astype(BF16)
        linked = jnp.minimum(jnp.dot(low, low, preferred_element_type=F32), 1.0)
    parts = jnp.concatenate(three_parts(log_gate), axis=0).astype(BF16)
    summed = jnp.dot(parts, linked.astype(BF16), preferred_element_type=F32)
    climb_ref[...] = summed[:8] + summed[8:16] + summed[16:]
    link_ref[...] = linked.T


def slot_token(lane):
    return jnp.where(lane % SLOTS < GROUP, (lane % 32) // SLOTS * GROUP + lane % SLOTS, -100000)


def placement(b, off, rows):
    lane = iota((rows, 128), 1)
    return (iota((rows, 128), 0) - off == slot_token(lane)) & (lane // 32 == b)


def attend_kernel(len_ref, acc_ref, g_ref, k_ref, v_ref, gate_ref, kout_ref, vout_ref, out_ref, q_ref, kt_ref, vt_ref, last_ref):
    b = pl.program_id(0)
    rows = k_ref.shape[1]
    start = lax.axis_index(KV) * rows

    @pl.when(b == 0)
    def _():
        q_ref[...] = g_ref[:, 0].astype(F32).reshape(512, 128).T
        kt_ref[...] = g_ref[:, 1].astype(F32).reshape(512, 128).astype(BF16)
        vt_ref[...] = g_ref[:, 2].astype(F32).reshape(512, 128).astype(BF16)
        lane = iota((8, 128), 1)
        total = jnp.zeros((8, 128), F32)
        for s in range(4):
            at = len_ref[s] + acc_ref[s] - 1 - start
            found = jnp.sum(jnp.where(iota((8, rows), 1) == at, gate_ref[s], 0.0), axis=1, keepdims=True)
            high, middle, low = three_parts(jnp.broadcast_to(found, (8, 128)))
            value = jnp.where(lane < 32, high, jnp.where(lane < 64, middle, low))
            here = (lane % 32 == s * 8 + iota((8, 128), 0)) & (lane < 96)
            total = total + jnp.where(here, value, 0.0)
        last_ref[...] = jnp.broadcast_to(jnp.sum(total, axis=0, keepdims=True), (8, 128))

    off = len_ref[b] + acc_ref[b] - start
    gates = gate_ref[b]
    seen = iota((64, rows), 1) < off
    lane = iota((64, 128), 1)
    half = lane < 64
    part = (lane % 64) // 8
    row = iota((64, 128), 0)
    mine = (lane % 8 == row % 8) & ((lane // 64) == (row // 32))
    slot = iota((4, 8, 128), 1)
    last = last_ref[...][None]
    for p in range(4):
        q = q_ref[pl.ds(b * 32, 32), p * 128 : (p + 1) * 128]
        both = jnp.concatenate([jnp.where(half[:32], q, 0.0), jnp.where(half[:32], 0.0, q)], axis=0).astype(BF16)
        scores = lax.dot_general(
            both, k_ref[0, :, p * 128 : (p + 1) * 128], NT, preferred_element_type=F32
        ) * 0.125
        shift = jnp.concatenate(
            [jnp.broadcast_to(gates[2 * p : 2 * p + 1], (32, rows)), jnp.broadcast_to(gates[2 * p + 1 : 2 * p + 2], (32, rows))],
            axis=0,
        )
        scores = jnp.where(seen, scores - shift, NEG_LARGE)
        highest = jnp.max(scores, axis=1, keepdims=True)
        weights = jnp.where(seen, jnp.exp(scores - highest), 0.0)
        total = jnp.sum(weights, axis=1, keepdims=True)
        weighted = jnp.dot(weights.astype(BF16), v_ref[0, :, p * 128 : (p + 1) * 128], preferred_element_type=F32)
        some = total > 0.0
        weighted = weighted * jnp.where(some, 1.0 / jnp.where(some, total, 1.0), 0.0)
        level = jnp.where(some, highest + jnp.log(jnp.where(some, total, 1.0)), NEG_LARGE)
        high, middle, low = three_parts(jnp.broadcast_to(level, (64, 128)))
        value = jnp.where(part == 0, high, jnp.where(part == 1, middle, low))
        value = jnp.where(mine & (part < 3), value, 0.0)
        levels = jnp.sum((value[:32] + value[32:]).reshape(4, 8, 128), axis=1, keepdims=True)
        pair = jnp.where(half[:32], weighted[:32], weighted[32:]).reshape(4, 8, 128)
        pair = jnp.where(slot == 6, levels, jnp.where(slot == 7, last, pair))
        out_ref[p * 4 : (p + 1) * 4, 0] = pair.astype(BF16)
    landing = (off > -24) & (off < rows)

    @pl.when(jnp.logical_not(landing))
    def _():
        kout_ref[...] = k_ref[...]
        vout_ref[...] = v_ref[...]

    @pl.when(landing)
    def _():
        placed = placement(b, off, rows).astype(F32).astype(BF16)
        index = iota((rows, 512), 0)
        landed = (index >= off) & (index < off + 24)
        for source, fresh, target in ((k_ref, kt_ref, kout_ref), (v_ref, vt_ref, vout_ref)):
            written = lax.dot_general(placed, fresh[...], NT, preferred_element_type=F32)
            target[0] = jnp.where(landed, written, source[0].astype(F32)).astype(BF16)


def merge_kernel(len_ref, acc_ref, r_ref, g_ref, climb_ref, link_ref, gate_ref, gain_ref, out_ref, gout_ref, qn_ref):
    rows = gate_ref.shape[2]
    index = lax.axis_index(KV)
    start = index * rows
    p = index // 16
    group = (index // 4) % 4
    seq = index % 4
    got = r_ref[...].astype(F32)
    lane3 = iota((64, 8, 128), 2)
    keep = (lane3 % 8 == iota((64, 8, 128), 1)) & ((lane3 % 64) // 8 < 3)
    level = jnp.where(keep, got[:, 6:7, :], 0.0).reshape(512, 128).astype(BF16)
    halves = (iota((128, 128), 0) // 64 == iota((128, 128), 1) // 64).astype(F32).astype(BF16)
    level = jnp.dot(level, halves, preferred_element_type=F32).reshape(64, 8, 128)
    top = jnp.max(level, axis=0)
    scale = jnp.exp(level - top[None])
    far_sum = jnp.sum(scale, axis=0)
    far = jnp.sum(scale * got, axis=0)
    last = jnp.sum(got, axis=0)[7:8]

    lane = iota((8, 128), 1)
    half = lane < 64
    lane1 = iota((1, 128), 1)
    first = seq * 8 + 2 * p
    pick = [
        jnp.sum(jnp.where((lane1 % 32 == first + k) & (lane1 < 96), last, 0.0), axis=1, keepdims=True)
        for k in range(2)
    ]
    top = top + jnp.where(half, pick[0], pick[1])

    at = pl.multiple_of(seq * 32 + group * 8, 8)
    qn_ref[...] = g_ref[pl.ds(p * 16, 16), 0].astype(F32).reshape(128, 128).T
    keys = g_ref[pl.ds(p * 16, 16), 1].astype(F32).reshape(128, 128).astype(BF16)
    values = g_ref[pl.ds(p * 16, 16), 2].astype(F32).reshape(128, 128).astype(BF16)
    q = qn_ref[pl.ds(at, 8), :]
    both = jnp.concatenate([jnp.where(half, q, 0.0), jnp.where(half, 0.0, q)], axis=0).astype(BF16)
    near = jnp.dot(both, keys, preferred_element_type=F32) * 0.125
    climb = climb_ref[...]
    head = iota((8, 128), 0)
    climbs = [jnp.sum(jnp.where(head == 2 * p + k, climb, 0.0), axis=0, keepdims=True) for k in range(2)]
    near = near - jnp.concatenate([jnp.broadcast_to(c, (8, 128)) for c in climbs], axis=0)
    linked = link_ref[pl.ds(at, 8), :]
    linked = jnp.concatenate([linked, linked], axis=0) > 0.5
    near = jnp.where(linked, near, NEG_LARGE)
    near_top = jnp.max(near, axis=1, keepdims=True)
    near = jnp.where(linked, jnp.exp(near - near_top), 0.0)
    near_sum = jnp.sum(near, axis=1, keepdims=True)
    near = lax.dot_general(near.astype(BF16), values, NT, preferred_element_type=F32)
    near = jnp.where(half, near[:8], near[8:])
    near_top = jnp.where(half, near_top[:8], near_top[8:])
    near_sum = jnp.where(half, near_sum[:8], near_sum[8:])
    overall = jnp.maximum(top, near_top)
    far_scale = jnp.exp(top - overall)
    near_scale = jnp.exp(near_top - overall)
    attended = (far * far_scale + near * near_scale) / (far_sum * far_scale + near_sum * near_scale)
    square = attended * attended
    low = jnp.sum(jnp.where(half, square, 0.0), axis=1, keepdims=True)
    high = jnp.sum(jnp.where(half, 0.0, square), axis=1, keepdims=True)
    mean = jnp.where(half, low, high) * (1.0 / 64.0)
    gain = jnp.sum(jnp.where(iota((4, 128), 0) == p, gain_ref[...].astype(F32), 0.0), axis=0, keepdims=True)
    heads = (attended * lax.rsqrt(mean + EPSILON) * gain).astype(BF16)
    out_ref[...] = jnp.broadcast_to(heads[None], out_ref.shape)

    lane32 = iota((32, 128), 1)
    column = jnp.sum(
        jnp.where((lane32 % 32 == iota((32, 128), 0)) & (lane32 < 96), last, 0.0), axis=1, keepdims=True
    )
    parts = jnp.concatenate(three_parts(climb), axis=0).astype(BF16)
    for b in range(4):
        off = len_ref[b] + acc_ref[b] - start
        placed = placement(b, off, rows).astype(F32).astype(BF16)
        written = lax.dot_general(parts, placed, NT, preferred_element_type=F32)
        written = written[:8] + written[8:16] + written[16:] + column[b * 8 : (b + 1) * 8]
        spot = iota((8, rows), 1)
        gout_ref[b] = jnp.where((spot >= off) & (spot < off + 24), written, gate_ref[b])


def mix_kernel(g_ref, w_ref, out_ref):
    total = jnp.zeros((32, 128), F32)
    for p in range(4):
        heads = g_ref[p * 16 : (p + 1) * 16].astype(F32).reshape(128, 128).astype(BF16)
        total = total + lax.dot_general(w_ref[:, p * 128 : (p + 1) * 128], heads, NT, preferred_element_type=F32)
    out_ref[...] = total.reshape(out_ref.shape)


def finish_kernel(x_ref, out_ref):
    total = x_ref[0]
    for k in range(1, x_ref.shape[0]):
        total = total + x_ref[k]
    turned = total.T
    for g in range(4):
        for b in range(4):
            at = (g * 4 + b) * SLOTS
            out_ref[b, g * GROUP : (g + 1) * GROUP, :] = turned[at : at + GROUP]


def spread(array, axis):
    return lax.all_to_all(array, axis, split_axis=0, concat_axis=0, tiled=True)


def local(
    tokens,
    norm_gain,
    w_query,
    w_key,
    w_value,
    w_forget,
    forget_bias,
    head_gain,
    w_out,
    cache_keys,
    cache_values,
    cache_gates,
    lengths,
    accepted,
    parents,
):
    rows = cache_keys.shape[1]
    pair_count = lax.axis_size("tp")
    smem = pl.BlockSpec(memory_space=pltpu.SMEM)
    vmem = pl.BlockSpec(memory_space=pltpu.VMEM)
    kernel = lambda body, **kw: pl.pallas_call(body, interpret=INTERPRET, **kw)

    packed = kernel(pack_kernel, out_shape=jax.ShapeDtypeStruct((64, 8, 128), BF16))(
        w_query, w_key, w_value, w_forget.T
    )
    columns = spread(packed, KV)

    groups = parents.reshape(4, 4, GROUP)
    groups = jnp.where(
        groups < 0, -1, groups // GROUP * SLOTS + groups % GROUP + 32 * jnp.arange(4, dtype=jnp.int32)[:, None, None]
    )
    slots = jnp.pad(groups, ((0, 0), (0, 0), (0, SLOTS - GROUP)), constant_values=-1).reshape(1, 128)
    pieces, climb, link = kernel(
        project_kernel,
        out_shape=(
            jax.ShapeDtypeStruct((64, 3, 8, 128), BF16),
            jax.ShapeDtypeStruct((8, 128), F32),
            jax.ShapeDtypeStruct((128, 128), F32),
        ),
        scratch_shapes=[pltpu.VMEM((32, 2048), F32), pltpu.VMEM((128, 2048), F32)],
    )(columns, tokens, norm_gain.reshape(1, -1), forget_bias.reshape(8, 1), slots)
    gathered = spread(pieces, KV)

    cache_spec = pl.BlockSpec((1, rows, 512), lambda b: (b, 0, 0))
    keys_out, values_out, partial = kernel(
        attend_kernel,
        grid=(4,),
        in_specs=[smem, smem, vmem, cache_spec, cache_spec, vmem],
        out_specs=(cache_spec, cache_spec, pl.BlockSpec((16, 1, 8, 128), lambda b: (0, b, 0, 0))),
        out_shape=(
            jax.ShapeDtypeStruct(cache_keys.shape, BF16),
            jax.ShapeDtypeStruct(cache_values.shape, BF16),
            jax.ShapeDtypeStruct((16, 4, 8, 128), BF16),
        ),
        scratch_shapes=[
            pltpu.VMEM((128, 512), F32),
            pltpu.VMEM((512, 128), BF16),
            pltpu.VMEM((512, 128), BF16),
            pltpu.VMEM((8, 128), F32),
        ],
    )(lengths, accepted, gathered, cache_keys, cache_values, cache_gates)
    received = spread(partial.reshape(64, 8, 128), KV)

    heads, gates_out = kernel(
        merge_kernel,
        in_specs=[smem, smem] + [vmem] * 6,
        out_shape=(
            jax.ShapeDtypeStruct((64, 8, 128), BF16),
            jax.ShapeDtypeStruct(cache_gates.shape, F32),
        ),
        scratch_shapes=[pltpu.VMEM((128, 128), F32)],
    )(lengths, accepted, received, gathered, climb, link, cache_gates, head_gain.reshape(4, 128))
    everyone = spread(heads, KV)

    share = kernel(mix_kernel, out_shape=jax.ShapeDtypeStruct((pair_count, 32 // pair_count, 128), F32))(
        everyone, w_out.T
    )
    summed = spread(share, "tp")
    mixed = kernel(finish_kernel, out_shape=jax.ShapeDtypeStruct((4, 24, 32 // pair_count), F32))(summed)
    return (mixed, keys_out, values_out, gates_out)


def solution(mesh):
    torus = Mesh(
        mesh.devices.reshape(mesh.shape["dp"], 16, 4, mesh.shape["tp"]),
        ("dp", "kv_0", "kv_1", "tp"),
    )
    return jax.shard_map(
        local,
        mesh=torus,
        in_specs=(
            P("dp", None, None),
            P(),
            P(KV, "tp"),
            P(KV, "tp"),
            P(KV, "tp"),
            P(KV, "tp"),
            P("tp"),
            P("tp"),
            P("tp", KV),
            P("dp", KV, "tp"),
            P("dp", KV, "tp"),
            P("dp", "tp", KV),
            P("dp"),
            P("dp"),
            P("dp", None),
        ),
        out_specs=(P("dp", None, KV_TP), P("dp", KV, "tp"), P("dp", KV, "tp"), P("dp", "tp", KV)),
        check_vma=False,
    )
```

time: 347 us -> 138 us (0.40)
  waiting for transfers between devices: 162 us -> 12 us
  local copies, waits for them, and re-layouts: 68.7 us -> 5.11 us
  matrix products: 19.6 us -> 0 us
  starting transfers between devices: 0.08 us -> 19.4 us
  Pallas kernels: 0 us -> 16.7 us
  blocking collectives: 66.7 us -> 83.2 us
  between operations: 14.9 us -> 0.67 us
  other arithmetic: 13.9 us -> 0.1 us
    all_gather x2 -> x0, waiting for transfers between devices: 162 us -> none  [the longest x1 104 us: in_one_piece(): whole = lax.all_gather(both, axis, axis=dim, tiled=True)]
    all_to_all x1 -> x4, blocking collectives: 16 us -> 83.2 us  [spread(): return lax.all_to_all(array, axis, split_axis=0, concat_axis=0, tiled=True)]
    mul x61 -> x0, local copies, waits for them, and re-layouts: 45.8 us -> none  [the longest x30 26 us: merge_pair(): second_part[2].reshape(seq_count, prop_count, head_count, -1)]
    psum x2 -> x0, blocking collectives: 39.6 us -> none  [one_axis_at_a_time(): array = lax.psum(array, axis)]
    dot_general x16 -> x0, matrix products: 19.6 us -> none  [the longest x4 7.6 us: local(): jnp.dot(normed, piece, preferred_element_type=jnp.float32)]
    all_to_all x0 -> x1, starting transfers between devices: none -> 19.4 us  [spread(): return lax.all_to_all(array, axis, split_axis=0, concat_axis=0, tiled=True)]
    pallas_call x0 -> x6, Pallas kernels: none -> 16.7 us  [the longest x1 6.84 us: local(): kernel(attend_kernel, grid=(4,), in_specs=[smem, smem, vmem, cache_spec,...]
    all_to_all x0 -> x1, waiting for transfers between devices: none -> 12 us  [spread(): return lax.all_to_all(array, axis, split_axis=0, concat_axis=0, tiled=True)]
  transfers between devices with their start and end apart: 2 -> 1, of which waited for: 2 -> 1; matrix products, arithmetic and copies ran while one was open for 6% -> 2% of each run, Pallas kernels for 0% -> 0%
where the time goes in v1:
time: 138 us; the launch traced here: 137 us
  blocking collectives  83.2 us (60%)
  starting transfers between devices  19.4 us (14%)
  Pallas kernels  16.7 us (12%)
  waiting for transfers between devices  12 us (9%)
  local copies, waits for them, and re-layouts  5.11 us (4%)
    all_to_all x4, blocking collectives, spread(): return lax.all_to_all(array, axis, split_axis=0, concat_axis=0, tiled=True)  83.2 us
    all_to_all x1, starting transfers between devices, spread(): return lax.all_to_all(array, axis, split_axis=0, concat_axis=0, tiled=True)  19.4 us
    all_to_all x1, waiting for transfers between devices, spread(): return lax.all_to_all(array, axis, split_axis=0, concat_axis=0, tiled=True)  12 us
    pallas_call x1, Pallas kernels, local(): kernel(attend_kernel, grid=(4,), in_specs=[smem, smem, vmem, cache_spec,...  6.84 us
    pallas_call x1, Pallas kernels, local(): kernel(project_kernel, out_shape=(jax.ShapeDtypeStruct((64, 3, 8, 128), B...  2.89 us
    unnamed x9, local copies, waits for them, and re-layouts  2.86 us
  transfers between devices with their start and end apart: 1, of which 1 were waited for; matrix products, arithmetic and copies ran while one was open for 2% of the time, Pallas kernels for 0%

profile of v1, /device:TPU:1, one launch (start us, length us, event | category | flops | bytes accessed | tf_op | source)
XLA Modules:
  0.0 137.1 jit_solution(10539456256441508221)
XLA Ops:
  0.6 1.6 %shard_map.174 = bf16[64,8,128]{2,1,0:T(8,128)(2,1)} custom-call(bf16[32,512]{1,0:T(8,128)(2,1)} %wq_ref.1, bf16[32,512]{1,0:T(8,128)(2,1)} %wk_ref.1, bf16[32,512]{1,0:T(8,128)(2,1)} %wv_ref.1, bf16[8,32]{1,0:T(8,128)(2,1)} %bitcast.7), custom_call_target="tpu_custom_call" | custom-call | tf_op jit(solution)/shard_map/pallas_call | solution.py:289
  2.2 0.0 copy-start.1
  2.2 19.4 %all-to-all-start = ((bf16[64,8,128]{2,1,0:T(8,128)(2,1)}), bf16[64,8,128]{2,1,0:T(8,128)(2,1)S(1)}, u32[]{:S(2)}, u32[]{:S(2)}) async-start(bf16[64,8,128]{2,1,0:T(8,128)(2,1)} %shard_map.174), calls=%async_computation | async-start | bytes 262144 | tf_op jit(solution)/shard_map/all_to_all | solution.py:263
  21.6 0.0 copy-done.1
  21.7 0.1 ne.25
  21.7 0.1 lt.19
  21.8 0.0 copy-start.3
  21.8 0.7 copy-done.3
  22.5 0.7 copy.19.bias_ref
  23.2 0.1 rem.19
  23.3 0.1 div.10
  23.3 0.1 fusion.3
  23.4 0.0 copy-start.2
  23.4 0.6 reshape.40.par_ref
  24.1 0.1 copy-done.2
  24.1 0.6 reshape.38.gain_ref
  24.7 12.0 %all-to-all-done.x_ref = bf16[64,8,128]{2,1,0:T(8,128)(2,1)S(1)} async-done(((bf16[64,8,128]{2,1,0:T(8,128)(2,1)}), bf16[64,8,128]{2,1,0:T(8,128)(2,1)S(1)}, u32[]{:S(2)}, u32[]{:S(2)}) %all-to-all-start) | async-done | bytes 131104 | tf_op jit(solution)/shard_map/all_to_all | solution.py:263
  36.7 0.0 copy-start
  36.7 0.7 copy-done
  37.3 2.9 %shard_map.175 = (bf16[64,3,8,128]{3,2,1,0:T(8,128)(2,1)}, f32[8,128]{1,0:T(8,128)}, f32[128,128]{1,0:T(8,128)}) custom-call(bf16[64,8,128]{2,1,0:T(8,128)(2,1)} %copy-done, bf16[4,24,2048]{2,1,0:T(8,128)(2,1)} %tok_ref.1, bf16[1,2048]{1,0:T(2,128)(2,1)} %reshape.38.gain_ref, f32[8,1]{1,0:T(8,128)} %copy.19.bias_ref, s32[1,128]{1,0:T(1,128)} %reshape.40.par_ref), custom_call_target="tpu_custom_call" | custom-call | tf_op jit(solution)/shard_map/pallas_call | solution.py:299
  40.2 29.8 %all_to_all.25.g_ref = bf16[64,3,8,128]{3,2,1,0:T(8,128)(2,1)} all-to-all(bf16[64,3,8,128]{3,2,1,0:T(8,128)(2,1)} %get-tuple-element.12), channel_id=1, replica_groups=mesh['dp'=4,'kv_0'=16,'kv_1'=4,'tp'=2] {'kv_0','kv_1'}, dimensions={0} | all-to-all | bytes 786432 | tf_op jit(solution)/shard_map/all_to_all | solution.py:263
  70.0 6.8 %shard_map.176 = (bf16[4,256,512]{2,1,0:T(8,128)(2,1)}, bf16[4,256,512]{2,1,0:T(8,128)(2,1)}, bf16[16,4,8,128]{3,2,1,0:T(8,128)(2,1)}) custom-call(s32[4]{0:T(128)} %len_ref.3, s32[4]{0:T(128)} %acc_ref.3, bf16[64,3,8,128]{3,2,1,0:T(8,128)(2,1)} %all_to_all.25.g_ref, bf16[4,256,512]{2,1,0:T(8,128)(2,1)} %k_ref.1, bf16[4,256,512]{2,1,0:T(8,128)(2,1)} %v_ref.1, ...), custom_call_target="tpu_custom_call" | custom-call | tf_op jit(solution)/shard_map/pallas_call | solution.py:311
  76.8 23.2 %all_to_all.26.r_ref = bf16[64,8,128]{2,1,0:T(8,128)(2,1)} all-to-all(bf16[64,8,128]{2,1,0:T(8,128)(2,1)} %bitcast.5), channel_id=1, replica_groups=mesh['dp'=4,'kv_0'=16,'kv_1'=4,'tp'=2] {'kv_0','kv_1'}, dimensions={0} | all-to-all | bytes 262144 | tf_op jit(solution)/shard_map/all_to_all | solution.py:263
  100.0 2.3 %shard_map.177 = (bf16[64,8,128]{2,1,0:T(8,128)(2,1)}, f32[4,8,256]{2,1,0:T(8,128)}) custom-call(s32[4]{0:T(128)} %len_ref.3, s32[4]{0:T(128)} %acc_ref.3, bf16[64,8,128]{2,1,0:T(8,128)(2,1)} %all_to_all.26.r_ref, bf16[64,3,8,128]{3,2,1,0:T(8,128)(2,1)} %all_to_all.25.g_ref, f32[8,128]{1,0:T(8,128)} %get-tuple-element.14.climb_ref, ...), custom_call_target="tpu_custom_call" | custom-call | tf_op jit(solution)/shard_map/pallas_call | solution.py:330
  102.3 20.5 %all_to_all.27.g_ref = bf16[64,8,128]{2,1,0:T(8,128)(2,1)} all-to-all(bf16[64,8,128]{2,1,0:T(8,128)(2,1)} %get-tuple-element.16), channel_id=1, replica_groups=mesh['dp'=4,'kv_0'=16,'kv_1'=4,'tp'=2] {'kv_0','kv_1'}, dimensions={0} | all-to-all | bytes 262144 | tf_op jit(solution)/shard_map/all_to_all | solution.py:263
  122.8 1.7 %shard_map.178 = f32[2,16,128]{2,1,0:T(8,128)} custom-call(bf16[64,8,128]{2,1,0:T(8,128)(2,1)} %all_to_all.27.g_ref, bf16[32,512]{1,0:T(8,128)(2,1)} %bitcast.6), custom_call_target="tpu_custom_call" | custom-call | tf_op jit(solution)/shard_map/pallas_call | solution.py:341
  124.5 9.7 %all_to_all.28.x_ref = f32[2,16,128]{2,1,0:T(8,128)} all-to-all(f32[2,16,128]{2,1,0:T(8,128)} %shard_map.178), channel_id=1, replica_groups=mesh['dp'=4,'kv_0'=16,'kv_1'=4,'tp'=2] {'tp'}, dimensions={0} | all-to-all | bytes 32768 | tf_op jit(solution)/shard_map/all_to_all | solution.py:263
  134.2 1.4 %shard_map.179 = f32[4,24,16]{2,1,0:T(8,128)} custom-call(f32[2,16,128]{2,1,0:T(8,128)} %all_to_all.28.x_ref), custom_call_target="tpu_custom_call" | custom-call | tf_op jit(solution)/shard_map/pallas_call | solution.py:345
  135.6 1.5 %copy.20 = f32[4,24,16]{1,2,0:T(8,128)} copy(f32[4,24,16]{2,1,0:T(8,128)} %shard_map.179) | data formatting | bytes 12288
  (4 shorter events, 0.0 us)
Async XLA Ops:
  2.2 19.4 %copy-start.1 = (s32[4,24]{1,0:T(4,128)S(1)}, s32[4,24]{1,0:T(4,128)}, u32[]{:S(2)}) copy-start(s32[4,24]{1,0:T(4,128)} %param.29) | copy-start | bytes 1156
  2.2 34.5 %all-to-all-start = ((bf16[64,8,128]{2,1,0:T(8,128)(2,1)}), bf16[64,8,128]{2,1,0:T(8,128)(2,1)S(1)}, u32[]{:S(2)}, u32[]{:S(2)}) async-start(bf16[64,8,128]{2,1,0:T(8,128)(2,1)} %shard_map.174), calls=%async_computation | async-start | bytes 262144 | tf_op jit(solution)/shard_map/all_to_all | solution.py:263
  21.8 0.7 copy-start.3
  23.4 0.7 copy-start.2
  36.7 0.7 copy-start

commit v2 on v1

v2 whole, which is shorter than its diff:
```python
import jax
import jax.numpy as jnp
from jax import lax
from jax.experimental import pallas as pl
from jax.experimental.pallas import tpu as pltpu
from jax.sharding import Mesh
from jax.sharding import PartitionSpec as P


KV = ("kv_0", "kv_1")
KV_TP = ("kv_0", "kv_1", "tp")

NEG_LARGE = -1e30
EPSILON = 1e-06
F32 = jnp.float32
BF16 = jnp.bfloat16

GROUP = 6
SLOTS = 8
NT = (((1,), (1,)), ((), ()))
INTERPRET = False


def iota(shape, dim):
    return lax.broadcasted_iota(jnp.int32, shape, dim)


def three_parts(x):
    high = x.astype(BF16).astype(F32)
    rest = x - high
    middle = rest.astype(BF16).astype(F32)
    return high, middle, rest - middle


def pack_kernel(wq_ref, wk_ref, wv_ref, wf_ref, out_ref):
    rows = wq_ref.shape[0]
    stacked = jnp.concatenate(
        [wq_ref[...].astype(F32), wk_ref[...].astype(F32), wv_ref[...].astype(F32), jnp.zeros((rows, wq_ref.shape[1]), F32)],
        axis=0,
    )
    turned = stacked.T.reshape(out_ref.shape)
    forget = jnp.concatenate([jnp.zeros((8, 3 * rows), F32), wf_ref[...].astype(F32)], axis=1)
    lane = iota((1, 8, 128), 2)
    out_ref[...] = jnp.where(lane >= 3 * rows, forget[None], turned).astype(BF16)


def normalize_kernel(tok_ref, gain_ref, par_ref, out_ref, link_ref, nrm_ref):
    nrm_ref[...] = jnp.zeros(nrm_ref.shape, F32)
    gain = gain_ref[...].astype(F32)
    for b in range(4):
        tok = tok_ref[b].astype(F32)
        normed = tok * lax.rsqrt(jnp.mean(tok * tok, axis=1, keepdims=True) + EPSILON) * gain
        for g in range(4):
            at = b * 32 + g * SLOTS
            nrm_ref[at : at + GROUP, :] = normed[g * GROUP : (g + 1) * GROUP]
    out_ref[...] = nrm_ref[...].astype(BF16)
    child = iota((128, 128), 0)
    linked = ((par_ref[...] == child) | (child == iota((128, 128), 1))).astype(F32)
    for _ in range(5):
        low = linked.astype(BF16)
        linked = jnp.minimum(jnp.dot(low, low, preferred_element_type=F32), 1.0)
    link_ref[...] = linked


def project_kernel(x_ref, nrm_ref, bias_ref, piece_ref, gate_ref, wt_ref):
    x = x_ref[...].astype(F32).reshape(16, 4, 8, 128)
    block = iota((128, 128), 1) // 32
    for t in range(4):
        row = None
        for n in range(4):
            moved = x[:, n].reshape(128, 128)
            if n != t:
                moved = pltpu.roll(moved, ((n - t) * 32) % 128, 1)
            row = moved if row is None else jnp.where(block == n, moved, row)
        row = row.reshape(16, 8, 128)
        for m in range(16):
            wt_ref[t * 8 : (t + 1) * 8, m * 128 : (m + 1) * 128] = row[m]
    out = lax.dot_general(wt_ref[...].astype(BF16), nrm_ref[...], NT, preferred_element_type=F32)
    piece = out[:24].reshape(3, 8, 128).astype(BF16)
    piece_ref[...] = jnp.broadcast_to(piece[None], piece_ref.shape)
    pre = out[24:] + bias_ref[...]
    gate_ref[...] = jnp.minimum(pre, 0.0) - jnp.log1p(jnp.exp(-jnp.abs(pre)))


def slot_token(lane):
    return jnp.where(lane % SLOTS < GROUP, (lane % 32) // SLOTS * GROUP + lane % SLOTS, -100000)


def placement(b, off, rows):
    lane = iota((rows, 128), 1)
    return (iota((rows, 128), 0) - off == slot_token(lane)) & (lane // 32 == b)


def columns_of(g_ref, n, start, count):
    parts = [g_ref[y, pl.ds(start, count), n].astype(F32) for y in range(4)]
    return jnp.stack(parts, axis=1).reshape(count * 32, 128)


def attend_kernel(len_ref, acc_ref, g_ref, k_ref, v_ref, gate_ref, out_ref, q_ref, last_ref):
    b = pl.program_id(0)
    rows = k_ref.shape[1]
    start = lax.axis_index(KV) * rows

    @pl.when(b == 0)
    def _():
        q_ref[...] = columns_of(g_ref, 0, 0, 16).T
        lane = iota((8, 128), 1)
        total = jnp.zeros((8, 128), F32)
        for s in range(4):
            at = len_ref[s] + acc_ref[s] - 1 - start
            found = jnp.sum(jnp.where(iota((8, rows), 1) == at, gate_ref[s], 0.0), axis=1, keepdims=True)
            high, middle, low = three_parts(jnp.broadcast_to(found, (8, 128)))
            value = jnp.where(lane < 32, high, jnp.where(lane < 64, middle, low))
            here = (lane % 32 == s * 8 + iota((8, 128), 0)) & (lane < 96)
            total = total + jnp.where(here, value, 0.0)
        last_ref[...] = jnp.broadcast_to(jnp.sum(total, axis=0, keepdims=True), (8, 128))

    off = len_ref[b] + acc_ref[b] - start
    gates = gate_ref[b]
    seen = iota((64, rows), 1) < off
    lane = iota((64, 128), 1)
    half = lane < 64
    part = (lane % 64) // 8
    row = iota((64, 128), 0)
    mine = (lane % 8 == row % 8) & ((lane // 64) == (row // 32))
    slot = iota((4, 8, 128), 1)
    last = last_ref[...][None]
    for p in range(4):
        q = q_ref[pl.ds(b * 32, 32), p * 128 : (p + 1) * 128]
        both = jnp.concatenate([jnp.where(half[:32], q, 0.0), jnp.where(half[:32], 0.0, q)], axis=0).astype(BF16)
        scores = lax.dot_general(
            both, k_ref[0, :, p * 128 : (p + 1) * 128], NT, preferred_element_type=F32
        ) * 0.125
        shift = jnp.concatenate(
            [jnp.broadcast_to(gates[2 * p : 2 * p + 1], (32, rows)), jnp.broadcast_to(gates[2 * p + 1 : 2 * p + 2], (32, rows))],
            axis=0,
        )
        scores = jnp.where(seen, scores - shift, NEG_LARGE)
        highest = jnp.max(scores, axis=1, keepdims=True)
        weights = jnp.where(seen, jnp.exp(scores - highest), 0.0)
        total = jnp.sum(weights, axis=1, keepdims=True)
        weighted = jnp.dot(weights.astype(BF16), v_ref[0, :, p * 128 : (p + 1) * 128], preferred_element_type=F32)
        some = total > 0.0
        weighted = weighted * jnp.where(some, 1.0 / jnp.where(some, total, 1.0), 0.0)
        level = jnp.where(some, highest + jnp.log(jnp.where(some, total, 1.0)), NEG_LARGE)
        high, middle, low = three_parts(jnp.broadcast_to(level, (64, 128)))
        value = jnp.where(part == 0, high, jnp.where(part == 1, middle, low))
        value = jnp.where(mine & (part < 3), value, 0.0)
        levels = jnp.sum((value[:32] + value[32:]).reshape(4, 8, 128), axis=1, keepdims=True)
        pair = jnp.where(half[:32], weighted[:32], weighted[32:]).reshape(4, 8, 128)
        pair = jnp.where(slot == 6, levels, jnp.where(slot == 7, last, pair))
        out_ref[p * 4 : (p + 1) * 4, 0] = pair.astype(BF16)


def write_kernel(len_ref, acc_ref, g_ref, k_ref, v_ref, kout_ref, vout_ref):
    b = pl.program_id(0)
    rows = k_ref.shape[1]
    off = len_ref[b] + acc_ref[b] - lax.axis_index(KV) * rows
    landing = (off > -24) & (off < rows)

    @pl.when(jnp.logical_not(landing))
    def _():
        kout_ref[...] = k_ref[...]
        vout_ref[...] = v_ref[...]

    @pl.when(landing)
    def _():
        placed = placement(b, off, rows).astype(F32).astype(BF16)
        index = iota((rows, 512), 0)
        landed = (index >= off) & (index < off + 24)
        for n, source, target in ((1, k_ref, kout_ref), (2, v_ref, vout_ref)):
            fresh = columns_of(g_ref, n, 0, 16).astype(BF16)
            written = lax.dot_general(placed, fresh, NT, preferred_element_type=F32)
            target[0] = jnp.where(landed, written, source[0].astype(F32)).astype(BF16)


def merger(index):
    return index // 16, (index // 4) % 4, index % 4


def climb_kernel(gate_ref, link_ref, climb_ref, turned_ref):
    link = link_ref[...]
    parts = jnp.concatenate(three_parts(gate_ref[...]), axis=0).astype(BF16)
    summed = jnp.dot(parts, link.astype(BF16), preferred_element_type=F32)
    climb_ref[...] = summed[:8] + summed[8:16] + summed[16:]
    turned_ref[...] = link.T


def near_kernel(g_ref, climb_ref, link_ref, out_ref, qn_ref):
    p, group, seq = merger(lax.axis_index(KV))
    half = iota((8, 128), 1) < 64
    at = pl.multiple_of(seq * 32 + group * 8, 8)
    climb = climb_ref[...]
    qn_ref[...] = columns_of(g_ref, 0, p * 4, 4).T
    keys = columns_of(g_ref, 1, p * 4, 4).astype(BF16)
    values = columns_of(g_ref, 2, p * 4, 4).astype(BF16)
    q = qn_ref[pl.ds(at, 8), :]
    both = jnp.concatenate([jnp.where(half, q, 0.0), jnp.where(half, 0.0, q)], axis=0).astype(BF16)
    near = jnp.dot(both, keys, preferred_element_type=F32) * 0.125
    head = iota((8, 128), 0)
    climbs = [jnp.sum(jnp.where(head == 2 * p + k, climb, 0.0), axis=0, keepdims=True) for k in range(2)]
    near = near - jnp.concatenate([jnp.broadcast_to(c, (8, 128)) for c in climbs], axis=0)
    linked = link_ref[pl.ds(at, 8), :]
    linked = jnp.concatenate([linked, linked], axis=0) > 0.5
    near = jnp.where(linked, near, NEG_LARGE)
    near_top = jnp.max(near, axis=1, keepdims=True)
    near = jnp.where(linked, jnp.exp(near - near_top), 0.0)
    near_sum = jnp.sum(near, axis=1, keepdims=True)
    near = lax.dot_general(near.astype(BF16), values, NT, preferred_element_type=F32)
    out_ref[0] = jnp.where(half, near[:8], near[8:])
    out_ref[1] = jnp.where(half, near_top[:8], near_top[8:])
    out_ref[2] = jnp.where(half, near_sum[:8], near_sum[8:])


def merge_kernel(r_ref, near_ref, gain_ref, out_ref, last_ref):
    p, _, seq = merger(lax.axis_index(KV))
    got = r_ref[...].astype(F32)
    lane3 = iota((64, 8, 128), 2)
    keep = (lane3 % 8 == iota((64, 8, 128), 1)) & ((lane3 % 64) // 8 < 3)
    level = jnp.where(keep, got[:, 6:7, :], 0.0).reshape(512, 128).astype(BF16)
    halves = (iota((128, 128), 0) // 64 == iota((128, 128), 1) // 64).astype(F32).astype(BF16)
    level = jnp.dot(level, halves, preferred_element_type=F32).reshape(64, 8, 128)
    top = jnp.max(level, axis=0)
    scale = jnp.exp(level - top[None])
    far_sum = jnp.sum(scale, axis=0)
    far = jnp.sum(scale * got, axis=0)
    whole = jnp.sum(got, axis=0)
    last_ref[...] = whole
    last = whole[7:8]

    half = iota((8, 128), 1) < 64
    lane1 = iota((1, 128), 1)
    first = seq * 8 + 2 * p
    pick = [
        jnp.sum(jnp.where((lane1 % 32 == first + k) & (lane1 < 96), last, 0.0), axis=1, keepdims=True)
        for k in range(2)
    ]
    top = top + jnp.where(half, pick[0], pick[1])
    near, near_top, near_sum = near_ref[0], near_ref[1], near_ref[2]
    overall = jnp.maximum(top, near_top)
    far_scale = jnp.exp(top - overall)
    near_scale = jnp.exp(near_top - overall)
    attended = (far * far_scale + near * near_scale) / (far_sum * far_scale + near_sum * near_scale)
    square = attended * attended
    low = jnp.sum(jnp.where(half, square, 0.0), axis=1, keepdims=True)
    high = jnp.sum(jnp.where(half, 0.0, square), axis=1, keepdims=True)
    mean = jnp.where(half, low, high) * (1.0 / 64.0)
    gain = jnp.sum(jnp.where(iota((4, 128), 0) == p, gain_ref[...].astype(F32), 0.0), axis=0, keepdims=True)
    heads = (attended * lax.rsqrt(mean + EPSILON) * gain).astype(BF16)
    out_ref[...] = jnp.broadcast_to(heads[None], out_ref.shape)


def gates_kernel(len_ref, acc_ref, last_ref, climb_ref, gate_ref, gout_ref):
    rows = gate_ref.shape[2]
    start = lax.axis_index(KV) * rows
    last = last_ref[...][7:8]
    lane = iota((32, 128), 1)
    column = jnp.sum(jnp.where((lane % 32 == iota((32, 128), 0)) & (lane < 96), last, 0.0), axis=1, keepdims=True)
    parts = jnp.concatenate(three_parts(climb_ref[...]), axis=0).astype(BF16)
    for b in range(4):
        off = len_ref[b] + acc_ref[b] - start
        placed = placement(b, off, rows).astype(F32).astype(BF16)
        written = lax.dot_general(parts, placed, NT, preferred_element_type=F32)
        written = written[:8] + written[8:16] + written[16:] + column[b * 8 : (b + 1) * 8]
        spot = iota((8, rows), 1)
        gout_ref[b] = jnp.where((spot >= off) & (spot < off + 24), written, gate_ref[b])


def mix_kernel(g_ref, w_ref, out_ref):
    total = jnp.zeros((32, 128), F32)
    for p in range(4):
        heads = g_ref[p * 16 : (p + 1) * 16].astype(F32).reshape(128, 128).astype(BF16)
        total = total + lax.dot_general(w_ref[:, p * 128 : (p + 1) * 128], heads, NT, preferred_element_type=F32)
    out_ref[...] = total.reshape(out_ref.shape)


def finish_kernel(x_ref, out_ref):
    total = x_ref[0]
    for k in range(1, x_ref.shape[0]):
        total = total + x_ref[k]
    for g in range(4):
        for b in range(4):
            at = (g * 4 + b) * SLOTS
            out_ref[b, :, g * GROUP : (g + 1) * GROUP] = total[:, at : at + GROUP]


def spread(array, axis):
    return lax.all_to_all(array, axis, split_axis=0, concat_axis=0, tiled=True)


def near_memory(shape, dtype):
    return pltpu.VMEM(shape, dtype)


def here(array):
    return pltpu.with_memory_space_constraint(array, pltpu.VMEM)


def step(
    tokens,
    norm_gain,
    w_query,
    w_key,
    w_value,
    w_forget,
    forget_bias,
    head_gain,
    w_out,
    cache_keys,
    cache_values,
    cache_gates,
    lengths,
    accepted,
    parents,
):
    rows = cache_keys.shape[1]
    pair_count = lax.axis_size("tp")
    smem = pl.BlockSpec(memory_space=pltpu.SMEM)
    vmem = pl.BlockSpec(memory_space=pltpu.VMEM)

    def kernel(body, out_shape, **kw):
        return pl.pallas_call(body, out_shape=out_shape, interpret=INTERPRET, **kw)

    packed = kernel(pack_kernel, near_memory((64, 8, 128), BF16))(w_query, w_key, w_value, w_forget.T)
    columns = spread(packed, KV)

    groups = parents.reshape(4, 4, GROUP)
    groups = jnp.where(
        groups < 0, -1, groups // GROUP * SLOTS + groups % GROUP + 32 * jnp.arange(4, dtype=jnp.int32)[:, None, None]
    )
    slots = jnp.pad(groups, ((0, 0), (0, 0), (0, SLOTS - GROUP)), constant_values=-1).reshape(1, 128)
    normed, link = kernel(
        normalize_kernel,
        (near_memory((128, 2048), BF16), near_memory((128, 128), F32)),
        scratch_shapes=[pltpu.VMEM((128, 2048), F32)],
    )(tokens, norm_gain.reshape(1, -1), slots)
    pieces, log_gate = kernel(
        project_kernel,
        (near_memory((16, 3, 8, 128), BF16), near_memory((8, 128), F32)),
        scratch_shapes=[pltpu.VMEM((32, 2048), F32)],
    )(here(columns), here(normed), forget_bias.reshape(8, 1))
    line = spread(pieces, KV[0])
    plane = spread(jnp.broadcast_to(line[None], (4, *line.shape)), KV[1])
    climb, turned = kernel(climb_kernel, (near_memory((8, 128), F32), near_memory((128, 128), F32)))(
        here(log_gate), here(link)
    )

    cache_spec = pl.BlockSpec((1, rows, 512), lambda b: (b, 0, 0))
    partial = kernel(
        attend_kernel,
        near_memory((16, 4, 8, 128), BF16),
        grid=(4,),
        in_specs=[smem, smem, vmem, cache_spec, cache_spec, vmem],
        out_specs=pl.BlockSpec((16, 1, 8, 128), lambda b: (0, b, 0, 0)),
        scratch_shapes=[pltpu.VMEM((128, 512), F32), pltpu.VMEM((8, 128), F32)],
    )(lengths, accepted, here(plane), cache_keys, cache_values, cache_gates)
    received = spread(partial.reshape(64, 8, 128), KV)
    keys_out, values_out = kernel(
        write_kernel,
        (
            jax.ShapeDtypeStruct(cache_keys.shape, BF16),
            jax.ShapeDtypeStruct(cache_values.shape, BF16),
        ),
        grid=(4,),
        in_specs=[smem, smem, vmem, cache_spec, cache_spec],
        out_specs=(cache_spec, cache_spec),
    )(lengths, accepted, here(plane), cache_keys, cache_values)
    near = kernel(
        near_kernel, near_memory((3, 8, 128), F32), scratch_shapes=[pltpu.VMEM((128, 128), F32)]
    )(here(plane), here(climb), here(turned))

    heads, last = kernel(
        merge_kernel,
        (near_memory((64, 8, 128), BF16), near_memory((8, 128), F32)),
    )(here(received), here(near), head_gain.reshape(4, 128))
    everyone = spread(heads, KV)
    gates_out = kernel(
        gates_kernel,
        jax.ShapeDtypeStruct(cache_gates.shape, F32),
        in_specs=[smem, smem] + [vmem] * 3,
    )(lengths, accepted, here(last), here(climb), cache_gates)

    share = kernel(mix_kernel, near_memory((pair_count, 32 // pair_count, 128), F32))(here(everyone), here(w_out.T))
    summed = spread(share, "tp")
    mixed = kernel(finish_kernel, jax.ShapeDtypeStruct((4, 32 // pair_count, 24), F32))(here(summed))
    mixed = jnp.swapaxes(mixed, 1, 2)
    return (mixed, keys_out, values_out, gates_out)


def solution(mesh):
    torus = Mesh(
        mesh.devices.reshape(mesh.shape["dp"], 16, 4, mesh.shape["tp"]),
        ("dp", "kv_0", "kv_1", "tp"),
    )
    return jax.shard_map(
        step,
        mesh=torus,
        in_specs=(
            P("dp", None, None),
            P(),
            P(KV, "tp"),
            P(KV, "tp"),
            P(KV, "tp"),
            P(KV, "tp"),
            P("tp"),
            P("tp"),
            P("tp", KV),
            P("dp", KV, "tp"),
            P("dp", KV, "tp"),
            P("dp", "tp", KV),
            P("dp"),
            P("dp"),
            P("dp", None),
        ),
        out_specs=(P("dp", None, KV_TP), P("dp", KV, "tp"), P("dp", KV, "tp"), P("dp", "tp", KV)),
        check_vma=False,
    )
```

time: 138 us -> 122 us (0.88)
  blocking collectives: 83.2 us -> 33.8 us
  waiting for transfers between devices: 12 us -> 34.2 us
  starting transfers between devices: 19.4 us -> 29.8 us
  Pallas kernels: 16.7 us -> 19.4 us
  local copies, waits for them, and re-layouts: 5.11 us -> 3.02 us
    all_to_all x4 -> x3, blocking collectives: 83.2 us -> 33.8 us  [spread(): return lax.all_to_all(array, axis, split_axis=0, concat_axis=0, tiled=True)]
    all_to_all x1 -> x3, waiting for transfers between devices: 12 us -> 34.2 us  [spread(): return lax.all_to_all(array, axis, split_axis=0, concat_axis=0, tiled=True)]
    all_to_all x1 -> x3, starting transfers between devices: 19.4 us -> 29.8 us  [spread(): return lax.all_to_all(array, axis, split_axis=0, concat_axis=0, tiled=True)]
    pallas_call x6 -> x11, Pallas kernels: 16.7 us -> 19.4 us  [the longest x1 6.34 us: step(): kernel(attend_kernel, near_memory((16, 4, 8, 128), BF16), grid=(4,), in_s...]
    unnamed x9 -> x8, local copies, waits for them, and re-layouts: 2.86 us -> 0.73 us
  transfers between devices with their start and end apart: 1 -> 3, of which waited for: 1 -> 3; matrix products, arithmetic and copies ran while one was open for 2% -> 2% of each run, Pallas kernels for 0% -> 7%
where the time goes in v2:
time: 122 us; the launch traced here: 121 us
  waiting for transfers between devices  34.2 us (28%)
  blocking collectives  33.8 us (28%)
  starting transfers between devices  29.8 us (24%)
  Pallas kernels  19.4 us (16%)
  local copies, waits for them, and re-layouts  3.02 us (2%)
    all_to_all x3, waiting for transfers between devices, spread(): return lax.all_to_all(array, axis, split_axis=0, concat_axis=0, tiled=True)  34.2 us
    all_to_all x3, blocking collectives, spread(): return lax.all_to_all(array, axis, split_axis=0, concat_axis=0, tiled=True)  33.8 us
    all_to_all x3, starting transfers between devices, spread(): return lax.all_to_all(array, axis, split_axis=0, concat_axis=0, tiled=True)  29.8 us
    pallas_call x1, Pallas kernels, step(): kernel(attend_kernel, near_memory((16, 4, 8, 128), BF16), grid=(4,), in_s...  6.34 us
    pallas_call x1, Pallas kernels, step(): kernel(write_kernel, (jax.ShapeDtypeStruct(cache_keys.shape, BF16), jax.S...  3.82 us
  transfers between devices with their start and end apart: 3, of which 3 were waited for; matrix products, arithmetic and copies ran while one was open for 2% of the time, Pallas kernels for 7%

profile of v2, /device:TPU:1, one launch (start us, length us, event | category | flops | bytes accessed | tf_op | source)
XLA Modules:
  0.0 121.0 jit_solution(12926620144200624164)
XLA Ops:
  0.6 1.6 %shard_map.174 = bf16[64,8,128]{2,1,0:T(8,128)(2,1)} custom-call(bf16[32,512]{1,0:T(8,128)(2,1)} %wq_ref.1, bf16[32,512]{1,0:T(8,128)(2,1)} %wk_ref.1, bf16[32,512]{1,0:T(8,128)(2,1)} %wv_ref.1, bf16[8,32]{1,0:T(8,128)(2,1)} %bitcast.8), custom_call_target="tpu_custom_call" | custom-call | tf_op jit(solution)/shard_map/pallas_call | solution.py:324
  2.2 19.4 %all-to-all-start = ((bf16[64,8,128]{2,1,0:T(8,128)(2,1)}), bf16[64,8,128]{2,1,0:T(8,128)(2,1)S(1)}, u32[]{:S(2)}, u32[]{:S(2)}) async-start(bf16[64,8,128]{2,1,0:T(8,128)(2,1)} %shard_map.174), calls=%async_computation | async-start | bytes 262144 | tf_op jit(solution)/shard_map/all_to_all | solution.py:288
  21.6 0.0 copy-start.1
  21.7 0.6 reshape.39.gain_ref
  22.3 0.1 copy-done.1
  22.3 0.1 lt.19
  22.4 0.1 div.10
  22.5 0.1 rem.19
  22.6 0.1 ne.25
  22.7 0.1 fusion.3
  22.8 0.6 reshape.40.par_ref
  23.4 0.7 copy-done.3
  24.0 0.7 copy.19.bias_ref
  24.7 1.9 %shard_map.175 = (bf16[128,2048]{1,0:T(8,128)(2,1)S(1)}, f32[128,128]{1,0:T(8,128)S(1)}) custom-call(bf16[4,24,2048]{2,1,0:T(8,128)(2,1)} %tok_ref.1, bf16[1,2048]{1,0:T(2,128)(2,1)} %reshape.39.gain_ref, s32[1,128]{1,0:T(1,128)} %reshape.40.par_ref), custom_call_target="tpu_custom_call" | custom-call | tf_op jit(solution)/shard_map/pallas_call | solution.py:332
  26.6 10.1 %all-to-all-done.x_ref = bf16[64,8,128]{2,1,0:T(8,128)(2,1)S(1)} async-done(((bf16[64,8,128]{2,1,0:T(8,128)(2,1)}), bf16[64,8,128]{2,1,0:T(8,128)(2,1)S(1)}, u32[]{:S(2)}, u32[]{:S(2)}) %all-to-all-start) | async-done | bytes 131104 | tf_op jit(solution)/shard_map/all_to_all | solution.py:288
  36.7 1.0 shard_map.176
  37.7 16.1 %all_to_all.30 = bf16[16,3,8,128]{3,2,1,0:T(8,128)(2,1)S(1)} all-to-all(bf16[16,3,8,128]{3,2,1,0:T(8,128)(2,1)S(1)} %get-tuple-element.15), channel_id=1, replica_groups=mesh['dp'=4,'kv_0'=16,'kv_1'=4,'tp'=2] {'kv_0'}, dimensions={0} | all-to-all | bytes 196608 | tf_op jit(solution)/shard_map/all_to_all | solution.py:288
  53.8 0.1 broadcast_in_dim.12
  53.9 8.6 %all_to_all.31.g_ref = bf16[4,16,3,8,128]{4,3,2,1,0:T(8,128)(2,1)S(1)} all-to-all(bf16[4,16,3,8,128]{4,3,2,1,0:T(8,128)(2,1)S(1)} %broadcast_in_dim.12), channel_id=1, replica_groups=mesh['dp'=4,'kv_0'=16,'kv_1'=4,'tp'=2] {'kv_1'}, dimensions={0} | all-to-all | bytes 786432 | tf_op jit(solution)/shard_map/all_to_all | solution.py:288
  62.5 6.3 %shard_map.177 = bf16[16,4,8,128]{3,2,1,0:T(8,128)(2,1)} custom-call(s32[4]{0:T(128)} %len_ref.5, s32[4]{0:T(128)} %acc_ref.5, bf16[4,16,3,8,128]{4,3,2,1,0:T(8,128)(2,1)S(1)} %all_to_all.31.g_ref, bf16[4,256,512]{2,1,0:T(8,128)(2,1)} %k_ref.3, bf16[4,256,512]{2,1,0:T(8,128)(2,1)} %v_ref.3, f32[4,8,256]{2,1,0:T(8,128)} %gate_ref.3), custom_call_target="tpu_custom_call" | custom-call | tf_op jit(solution)/shard_map/pallas_call | solution.py:349
  68.8 5.8 %all-to-all-start.3 = ((bf16[64,8,128]{2,1,0:T(8,128)(2,1)}), bf16[64,8,128]{2,1,0:T(8,128)(2,1)S(1)}, u32[]{:S(2)}, u32[]{:S(2)}) async-start(bf16[64,8,128]{2,1,0:T(8,128)(2,1)} %bitcast.2), calls=%async_computation.3 | async-start | bytes 262144 | tf_op jit(solution)/shard_map/all_to_all | solution.py:288
  74.6 0.1 shard_map.178
  74.7 0.4 shard_map.179.near_ref
  75.2 14.4 %all-to-all-done.3.r_ref = bf16[64,8,128]{2,1,0:T(8,128)(2,1)S(1)} async-done(((bf16[64,8,128]{2,1,0:T(8,128)(2,1)}), bf16[64,8,128]{2,1,0:T(8,128)(2,1)S(1)}, u32[]{:S(2)}, u32[]{:S(2)}) %all-to-all-start.3) | async-done | bytes 131104 | tf_op jit(solution)/shard_map/all_to_all | solution.py:288
  89.6 1.7 %shard_map.180 = (bf16[64,8,128]{2,1,0:T(8,128)(2,1)}, f32[8,128]{1,0:T(8,128)S(1)}) custom-call(bf16[64,8,128]{2,1,0:T(8,128)(2,1)S(1)} %all-to-all-done.3.r_ref, f32[3,8,128]{2,1,0:T(8,128)S(1)} %shard_map.179.near_ref, bf16[4,128]{1,0:T(4,128)(2,1)} %bitcast.9), custom_call_target="tpu_custom_call" | custom-call | tf_op jit(solution)/shard_map/pallas_call | solution.py:372
  91.3 4.6 %all-to-all-start.4 = ((bf16[64,8,128]{2,1,0:T(8,128)(2,1)}), bf16[64,8,128]{2,1,0:T(8,128)(2,1)S(1)}, u32[]{:S(2)}, u32[]{:S(2)}) async-start(bf16[64,8,128]{2,1,0:T(8,128)(2,1)} %get-tuple-element.20), calls=%async_computation.4 | async-start | bytes 262144 | tf_op jit(solution)/shard_map/all_to_all | solution.py:288
  95.9 3.8 %shard_map.183 = (bf16[4,256,512]{2,1,0:T(8,128)(2,1)}, bf16[4,256,512]{2,1,0:T(8,128)(2,1)}) custom-call(s32[4]{0:T(128)} %len_ref.5, s32[4]{0:T(128)} %acc_ref.5, bf16[4,16,3,8,128]{4,3,2,1,0:T(8,128)(2,1)S(1)} %all_to_all.31.g_ref, bf16[4,256,512]{2,1,0:T(8,128)(2,1)} %k_ref.3, bf16[4,256,512]{2,1,0:T(8,128)(2,1)} %v_ref.3), custom_call_target="tpu_custom_call" | custom-call | tf_op jit(solution)/shard_map/pallas_call | solution.py:358
  99.8 1.6 %shard_map.184 = f32[4,8,256]{2,1,0:T(8,128)} custom-call(s32[4]{0:T(128)} %len_ref.5, s32[4]{0:T(128)} %acc_ref.5, f32[8,128]{1,0:T(8,128)S(1)} %get-tuple-element.23.last_ref, f32[8,128]{1,0:T(8,128)S(1)} %get-tuple-element.18.climb_ref, f32[4,8,256]{2,1,0:T(8,128)} %gate_ref.3), custom_call_target="tpu_custom_call" | custom-call | tf_op jit(solution)/shard_map/pallas_call | solution.py:377
  101.4 9.7 %all-to-all-done.4.g_ref = bf16[64,8,128]{2,1,0:T(8,128)(2,1)S(1)} async-done(((bf16[64,8,128]{2,1,0:T(8,128)(2,1)}), bf16[64,8,128]{2,1,0:T(8,128)(2,1)S(1)}, u32[]{:S(2)}, u32[]{:S(2)}) %all-to-all-start.4) | async-done | bytes 131104 | tf_op jit(solution)/shard_map/all_to_all | solution.py:288
  111.1 0.2 shard_map.181
  111.2 9.1 %all_to_all.32.x_ref = f32[2,16,128]{2,1,0:T(8,128)S(1)} all-to-all(f32[2,16,128]{2,1,0:T(8,128)S(1)} %shard_map.181), channel_id=1, replica_groups=mesh['dp'=4,'kv_0'=16,'kv_1'=4,'tp'=2] {'tp'}, dimensions={0} | all-to-all | bytes 32768 | tf_op jit(solution)/shard_map/all_to_all | solution.py:288
  120.3 0.7 shard_map.182
  (9 shorter events, 0.0 us)
Async XLA Ops:
  2.2 19.4 %copy-start.2 = (bf16[2048]{0:T(1024)(128)(2,1)S(1)}, bf16[2048]{0:T(1024)(128)(2,1)}, u32[]{:S(2)}) copy-start(bf16[2048]{0:T(1024)(128)(2,1)} %param.16) | copy-start | bytes 12292
  2.2 34.5 %all-to-all-start = ((bf16[64,8,128]{2,1,0:T(8,128)(2,1)}), bf16[64,8,128]{2,1,0:T(8,128)(2,1)S(1)}, u32[]{:S(2)}, u32[]{:S(2)}) async-start(bf16[64,8,128]{2,1,0:T(8,128)(2,1)} %shard_map.174), calls=%async_computation | async-start | bytes 262144 | tf_op jit(solution)/shard_map/all_to_all | solution.py:288
  21.6 0.7 copy-start.1
  23.4 0.7 copy-start.3
  68.8 20.8 %all-to-all-start.3 = ((bf16[64,8,128]{2,1,0:T(8,128)(2,1)}), bf16[64,8,128]{2,1,0:T(8,128)(2,1)S(1)}, u32[]{:S(2)}, u32[]{:S(2)}) async-start(bf16[64,8,128]{2,1,0:T(8,128)(2,1)} %bitcast.2), calls=%async_computation.3 | async-start | bytes 262144 | tf_op jit(solution)/shard_map/all_to_all | solution.py:288
  91.3 19.8 %all-to-all-start.4 = ((bf16[64,8,128]{2,1,0:T(8,128)(2,1)}), bf16[64,8,128]{2,1,0:T(8,128)(2,1)S(1)}, u32[]{:S(2)}, u32[]{:S(2)}) async-start(bf16[64,8,128]{2,1,0:T(8,128)(2,1)} %get-tuple-element.20), calls=%async_computation.4 | async-start | bytes 262144 | tf_op jit(solution)/shard_map/all_to_all | solution.py:288
  99.7 11.3 %copy-start = (bf16[512,32]{0,1:T(8,128)(2,1)S(1)}, bf16[512,32]{0,1:T(8,128)(2,1)}, u32[]{:S(2)}) copy-start(bf16[512,32]{0,1:T(8,128)(2,1)} %param.23) | copy-start | bytes 98308

commit v3 on v2

v3 whole, which is shorter than its diff:
```python
import jax
import jax.numpy as jnp
from jax import lax
from jax.experimental import pallas as pl
from jax.experimental.pallas import tpu as pltpu
from jax.sharding import Mesh
from jax.sharding import PartitionSpec as P


KV = ("kv_0", "kv_1")
KV_TP = ("kv_0", "kv_1", "tp")

NEG_LARGE = -1e30
EPSILON = 1e-06
F32 = jnp.float32
BF16 = jnp.bfloat16

GROUP = 6
SLOTS = 8
NT = (((1,), (1,)), ((), ()))
INTERPRET = False


def iota(shape, dim):
    return lax.broadcasted_iota(jnp.int32, shape, dim)


def three_parts(x):
    high = x.astype(BF16).astype(F32)
    rest = x - high
    middle = rest.astype(BF16).astype(F32)
    return high, middle, rest - middle


def merger(index):
    return index // 16, (index // 4) % 4, index % 4


def pack_kernel(wq_ref, wk_ref, wv_ref, wf_ref, out_ref):
    rows = wq_ref.shape[0]
    stacked = jnp.concatenate(
        [wq_ref[...].astype(F32), wk_ref[...].astype(F32), wv_ref[...].astype(F32), jnp.zeros((rows, wq_ref.shape[1]), F32)],
        axis=0,
    )
    turned = stacked.T.reshape(out_ref.shape)
    forget = jnp.concatenate([jnp.zeros((8, 3 * rows), F32), wf_ref[...].astype(F32)], axis=1)
    lane = iota((1, 8, 128), 2)
    out_ref[...] = jnp.where(lane >= 3 * rows, forget[None], turned).astype(BF16)


def prepare_kernel(
    len_ref, acc_ref, tok_ref, gain_ref, par_ref, bias_ref, gate_ref, head_gain_ref,
    out_ref, link_ref, turned_ref, off_ref, last_ref, bias_out_ref, own_gain_ref, nrm_ref,
):
    rows = gate_ref.shape[2]
    index = lax.axis_index(KV)
    start = index * rows
    nrm_ref[...] = jnp.zeros(nrm_ref.shape, F32)
    gain = gain_ref[...].astype(F32)
    for b in range(4):
        tok = tok_ref[b].astype(F32)
        normed = tok * lax.rsqrt(jnp.mean(tok * tok, axis=1, keepdims=True) + EPSILON) * gain
        for g in range(4):
            at = b * 32 + g * SLOTS
            nrm_ref[at : at + GROUP, :] = normed[g * GROUP : (g + 1) * GROUP]
    out_ref[...] = nrm_ref[...].astype(BF16)

    child = iota((128, 128), 0)
    linked = ((par_ref[...] == child) | (child == iota((128, 128), 1))).astype(F32)
    for _ in range(5):
        low = linked.astype(BF16)
        linked = jnp.minimum(jnp.dot(low, low, preferred_element_type=F32), 1.0)
    link_ref[...] = linked
    turned_ref[...] = linked.T

    lane = iota((8, 128), 1)
    row = iota((8, 128), 0)
    total = jnp.zeros((8, 128), F32)
    offsets = jnp.zeros((8, 128), jnp.int32)
    for s in range(4):
        off = len_ref[s] + acc_ref[s] - start
        offsets = jnp.where(row == s, off, offsets)
        found = jnp.sum(jnp.where(iota((8, rows), 1) == off - 1, gate_ref[s], 0.0), axis=1, keepdims=True)
        high, middle, low = three_parts(jnp.broadcast_to(found, (8, 128)))
        value = jnp.where(lane < 32, high, jnp.where(lane < 64, middle, low))
        total = total + jnp.where((lane % 32 == s * 8 + row) & (lane < 96), value, 0.0)
    off_ref[...] = offsets
    last_ref[...] = jnp.broadcast_to(jnp.sum(total, axis=0, keepdims=True), (8, 128))
    bias_out_ref[...] = jnp.broadcast_to(bias_ref[...], (8, 128))
    own = jnp.where(iota((4, 128), 0) == merger(index)[0], head_gain_ref[...].astype(F32), 0.0)
    own_gain_ref[...] = jnp.broadcast_to(jnp.sum(own, axis=0, keepdims=True), (8, 128))


def project_kernel(x_ref, nrm_ref, bias_ref, piece_ref, gate_ref, wt_ref):
    x = x_ref[...].astype(F32).reshape(16, 4, 8, 128)
    block = iota((128, 128), 1) // 32
    for t in range(4):
        row = None
        for n in range(4):
            moved = x[:, n].reshape(128, 128)
            if n != t:
                moved = pltpu.roll(moved, ((n - t) * 32) % 128, 1)
            row = moved if row is None else jnp.where(block == n, moved, row)
        row = row.reshape(16, 8, 128)
        for m in range(16):
            wt_ref[t * 8 : (t + 1) * 8, m * 128 : (m + 1) * 128] = row[m]
    out = lax.dot_general(wt_ref[...].astype(BF16), nrm_ref[...], NT, preferred_element_type=F32)
    piece = out[:24].reshape(3, 8, 128).astype(BF16)
    piece_ref[...] = jnp.broadcast_to(piece[None], piece_ref.shape)
    pre = out[24:] + bias_ref[...]
    gate_ref[...] = jnp.minimum(pre, 0.0) - jnp.log1p(jnp.exp(-jnp.abs(pre)))


def slot_token(lane):
    return jnp.where(lane % SLOTS < GROUP, (lane % 32) // SLOTS * GROUP + lane % SLOTS, -100000)


def placement(b, off, rows):
    lane = iota((rows, 128), 1)
    return (iota((rows, 128), 0) - off == slot_token(lane)) & (lane // 32 == b)


def columns_of(g_ref, n, start, count):
    parts = [g_ref[y, pl.ds(start, count), n].astype(F32) for y in range(4)]
    return jnp.stack(parts, axis=1).reshape(count * 32, 128)


def attend_kernel(
    off_ref, last_ref, g_ref, k_ref, v_ref, gate_ref, lg_ref, link_ref, turned_ref,
    out_ref, near_ref, climb_ref, q_ref,
):
    rows = k_ref.shape[1]
    q_ref[...] = columns_of(g_ref, 0, 0, 16).T
    lane = iota((64, 128), 1)
    half = lane < 64
    part = (lane % 64) // 8
    row = iota((64, 128), 0)
    mine = (lane % 8 == row % 8) & ((lane // 64) == (row // 32))
    slot = iota((4, 8, 128), 1)
    last = last_ref[...][None]
    for b in range(4):
        gates = gate_ref[b]
        seen = iota((64, rows), 1) < off_ref[b : b + 1, 0:1]
        for p in range(4):
            q = q_ref[b * 32 : (b + 1) * 32, p * 128 : (p + 1) * 128]
            both = jnp.concatenate([jnp.where(half[:32], q, 0.0), jnp.where(half[:32], 0.0, q)], axis=0).astype(BF16)
            scores = lax.dot_general(
                both, k_ref[b, :, p * 128 : (p + 1) * 128], NT, preferred_element_type=F32
            ) * 0.125
            shift = jnp.concatenate(
                [jnp.broadcast_to(gates[2 * p + k : 2 * p + k + 1], (32, rows)) for k in range(2)], axis=0
            )
            scores = jnp.where(seen, scores - shift, NEG_LARGE)
            highest = jnp.max(scores, axis=1, keepdims=True)
            weights = jnp.where(seen, jnp.exp(scores - highest), 0.0)
            total = jnp.sum(weights, axis=1, keepdims=True)
            weighted = jnp.dot(
                weights.astype(BF16), v_ref[b, :, p * 128 : (p + 1) * 128], preferred_element_type=F32
            )
            some = total > 0.0
            weighted = weighted * jnp.where(some, 1.0 / jnp.where(some, total, 1.0), 0.0)
            level = jnp.where(some, highest + jnp.log(jnp.where(some, total, 1.0)), NEG_LARGE)
            high, middle, low = three_parts(jnp.broadcast_to(level, (64, 128)))
            value = jnp.where(part == 0, high, jnp.where(part == 1, middle, low))
            value = jnp.where(mine & (part < 3), value, 0.0)
            levels = jnp.sum((value[:32] + value[32:]).reshape(4, 8, 128), axis=1, keepdims=True)
            pair = jnp.where(half[:32], weighted[:32], weighted[32:]).reshape(4, 8, 128)
            pair = jnp.where(slot == 6, levels, jnp.where(slot == 7, last, pair))
            out_ref[p * 4 : (p + 1) * 4, b] = pair.astype(BF16)

    parts = jnp.concatenate(three_parts(lg_ref[...]), axis=0).astype(BF16)
    summed = jnp.dot(parts, link_ref[...].astype(BF16), preferred_element_type=F32)
    climb = summed[:8] + summed[8:16] + summed[16:]
    climb_ref[...] = climb
    p, group, seq = merger(lax.axis_index(KV))
    half = iota((8, 128), 1) < 64
    at = pl.multiple_of(seq * 32 + group * 8, 8)
    keys = columns_of(g_ref, 1, p * 4, 4).astype(BF16)
    values = columns_of(g_ref, 2, p * 4, 4).astype(BF16)
    q = q_ref[pl.ds(at, 8), pl.ds(pl.multiple_of(p * 128, 128), 128)]
    both = jnp.concatenate([jnp.where(half, q, 0.0), jnp.where(half, 0.0, q)], axis=0).astype(BF16)
    near = jnp.dot(both, keys, preferred_element_type=F32) * 0.125
    head = iota((8, 128), 0)
    climbs = [jnp.sum(jnp.where(head == 2 * p + k, climb, 0.0), axis=0, keepdims=True) for k in range(2)]
    near = near - jnp.concatenate([jnp.broadcast_to(c, (8, 128)) for c in climbs], axis=0)
    linked = turned_ref[pl.ds(at, 8), :]
    linked = jnp.concatenate([linked, linked], axis=0) > 0.5
    near = jnp.where(linked, near, NEG_LARGE)
    near_top = jnp.max(near, axis=1, keepdims=True)
    near = jnp.where(linked, jnp.exp(near - near_top), 0.0)
    near_sum = jnp.sum(near, axis=1, keepdims=True)
    near = lax.dot_general(near.astype(BF16), values, NT, preferred_element_type=F32)
    near_ref[0] = jnp.where(half, near[:8], near[8:])
    near_ref[1] = jnp.where(half, near_top[:8], near_top[8:])
    near_ref[2] = jnp.where(half, near_sum[:8], near_sum[8:])


def write_kernel(len_ref, acc_ref, g_ref, k_ref, v_ref, kout_ref, vout_ref):
    b = pl.program_id(0)
    rows = k_ref.shape[1]
    off = len_ref[b] + acc_ref[b] - lax.axis_index(KV) * rows
    landing = (off > -24) & (off < rows)

    @pl.when(jnp.logical_not(landing))
    def _():
        kout_ref[...] = k_ref[...]
        vout_ref[...] = v_ref[...]

    @pl.when(landing)
    def _():
        placed = placement(b, off, rows).astype(F32).astype(BF16)
        index = iota((rows, 512), 0)
        landed = (index >= off) & (index < off + 24)
        for n, source, target in ((1, k_ref, kout_ref), (2, v_ref, vout_ref)):
            fresh = columns_of(g_ref, n, 0, 16).astype(BF16)
            written = lax.dot_general(placed, fresh, NT, preferred_element_type=F32)
            target[0] = jnp.where(landed, written, source[0].astype(F32)).astype(BF16)


def merge_kernel(r_ref, near_ref, gain_ref, out_ref, last_ref):
    p, _, seq = merger(lax.axis_index(KV))
    got = r_ref[...].astype(F32)
    lane3 = iota((64, 8, 128), 2)
    keep = (lane3 % 8 == iota((64, 8, 128), 1)) & ((lane3 % 64) // 8 < 3)
    level = jnp.where(keep, got[:, 6:7, :], 0.0).reshape(512, 128).astype(BF16)
    halves = (iota((128, 128), 0) // 64 == iota((128, 128), 1) // 64).astype(F32).astype(BF16)
    level = jnp.dot(level, halves, preferred_element_type=F32).reshape(64, 8, 128)
    top = jnp.max(level, axis=0)
    scale = jnp.exp(level - top[None])
    far_sum = jnp.sum(scale, axis=0)
    far = jnp.sum(scale * got, axis=0)
    whole = jnp.sum(got, axis=0)
    last_ref[...] = whole
    last = whole[7:8]

    half = iota((8, 128), 1) < 64
    lane1 = iota((1, 128), 1)
    first = seq * 8 + 2 * p
    pick = [
        jnp.sum(jnp.where((lane1 % 32 == first + k) & (lane1 < 96), last, 0.0), axis=1, keepdims=True)
        for k in range(2)
    ]
    top = top + jnp.where(half, pick[0], pick[1])
    near, near_top, near_sum = near_ref[0], near_ref[1], near_ref[2]
    overall = jnp.maximum(top, near_top)
    far_scale = jnp.exp(top - overall)
    near_scale = jnp.exp(near_top - overall)
    attended = (far * far_scale + near * near_scale) / (far_sum * far_scale + near_sum * near_scale)
    square = attended * attended
    low = jnp.sum(jnp.where(half, square, 0.0), axis=1, keepdims=True)
    high = jnp.sum(jnp.where(half, 0.0, square), axis=1, keepdims=True)
    mean = jnp.where(half, low, high) * (1.0 / 64.0)
    heads = (attended * lax.rsqrt(mean + EPSILON) * gain_ref[...]).astype(BF16)
    out_ref[...] = jnp.broadcast_to(heads[None], out_ref.shape)


def gates_kernel(off_ref, last_ref, climb_ref, gate_ref, gout_ref):
    rows = gate_ref.shape[2]
    last = last_ref[...][7:8]
    lane = iota((32, 128), 1)
    column = jnp.sum(jnp.where((lane % 32 == iota((32, 128), 0)) & (lane < 96), last, 0.0), axis=1, keepdims=True)
    parts = jnp.concatenate(three_parts(climb_ref[...]), axis=0).astype(BF16)
    for b in range(4):
        off = off_ref[b : b + 1, 0:1]
        placed = placement(b, off, rows).astype(F32).astype(BF16)
        written = lax.dot_general(parts, placed, NT, preferred_element_type=F32)
        written = written[:8] + written[8:16] + written[16:] + column[b * 8 : (b + 1) * 8]
        spot = iota((8, rows), 1)
        gout_ref[b] = jnp.where((spot >= off) & (spot < off + 24), written, gate_ref[b])


def mix_kernel(g_ref, w_ref, out_ref):
    total = jnp.zeros((32, 128), F32)
    for p in range(4):
        heads = g_ref[p * 16 : (p + 1) * 16].astype(F32).reshape(128, 128).astype(BF16)
        total = total + lax.dot_general(w_ref[:, p * 128 : (p + 1) * 128], heads, NT, preferred_element_type=F32)
    out_ref[...] = total.reshape(out_ref.shape)


def finish_kernel(x_ref, out_ref):
    width = out_ref.shape[1]
    own = pl.multiple_of(lax.axis_index("tp") * width, width)
    total = x_ref[0, pl.ds(own, width), :]
    for k in range(1, x_ref.shape[0]):
        total = total + x_ref[k, pl.ds(own, width), :]
    for g in range(4):
        for b in range(4):
            at = (g * 4 + b) * SLOTS
            out_ref[b, :, g * GROUP : (g + 1) * GROUP] = total[:, at : at + GROUP]


def spread(array, axis):
    return lax.all_to_all(array, axis, split_axis=0, concat_axis=0, tiled=True)


def near_memory(shape, dtype):
    return pltpu.VMEM(shape, dtype)


def here(array):
    return pltpu.with_memory_space_constraint(array, pltpu.VMEM)


def step(
    tokens,
    norm_gain,
    w_query,
    w_key,
    w_value,
    w_forget,
    forget_bias,
    head_gain,
    w_out,
    cache_keys,
    cache_values,
    cache_gates,
    lengths,
    accepted,
    parents,
):
    rows = cache_keys.shape[1]
    pair_count = lax.axis_size("tp")
    smem = pl.BlockSpec(memory_space=pltpu.SMEM)
    vmem = pl.BlockSpec(memory_space=pltpu.VMEM)

    def kernel(body, out_shape, **kw):
        return pl.pallas_call(body, out_shape=out_shape, interpret=INTERPRET, **kw)

    packed = kernel(pack_kernel, near_memory((64, 8, 128), BF16))(w_query, w_key, w_value, w_forget.T)
    columns = spread(packed, KV)

    groups = parents.reshape(4, 4, GROUP)
    groups = jnp.where(
        groups < 0, -1, groups // GROUP * SLOTS + groups % GROUP + 32 * jnp.arange(4, dtype=jnp.int32)[:, None, None]
    )
    slots = jnp.pad(groups, ((0, 0), (0, 0), (0, SLOTS - GROUP)), constant_values=-1).reshape(1, 128)
    gates = here(cache_gates)
    keys = here(cache_keys)
    values = here(cache_values)
    small = near_memory((8, 128), F32)
    normed, link, turned, offsets, last_part, bias, own_gain = kernel(
        prepare_kernel,
        (
            near_memory((128, 2048), BF16),
            near_memory((128, 128), F32),
            near_memory((128, 128), F32),
            near_memory((8, 128), jnp.int32),
            small,
            small,
            small,
        ),
        in_specs=[smem, smem] + [vmem] * 6,
        scratch_shapes=[pltpu.VMEM((128, 2048), F32)],
    )(
        lengths,
        accepted,
        tokens,
        norm_gain.reshape(1, -1),
        slots,
        forget_bias.reshape(8, 1),
        gates,
        head_gain.reshape(4, 128),
    )
    pieces, log_gate = kernel(
        project_kernel,
        (near_memory((16, 3, 8, 128), BF16), small),
        scratch_shapes=[pltpu.VMEM((32, 2048), F32)],
    )(here(columns), here(normed), here(bias))
    line = spread(pieces, KV[0])
    plane = here(spread(jnp.broadcast_to(line[None], (4, *line.shape)), KV[1]))

    partial, near, climb = kernel(
        attend_kernel,
        (near_memory((16, 4, 8, 128), BF16), near_memory((3, 8, 128), F32), small),
        scratch_shapes=[pltpu.VMEM((128, 512), F32)],
    )(
        here(offsets),
        here(last_part),
        plane,
        keys,
        values,
        gates,
        here(log_gate),
        here(link),
        here(turned),
    )
    received = spread(partial.reshape(64, 8, 128), KV)
    heads, last = kernel(merge_kernel, (near_memory((64, 8, 128), BF16), small))(
        here(received), here(near), here(own_gain)
    )
    everyone = spread(heads, KV)
    cache_spec = pl.BlockSpec((1, rows, 512), lambda b: (b, 0, 0))
    keys_out, values_out = kernel(
        write_kernel,
        (
            jax.ShapeDtypeStruct(cache_keys.shape, BF16),
            jax.ShapeDtypeStruct(cache_values.shape, BF16),
        ),
        grid=(4,),
        in_specs=[smem, smem, vmem, cache_spec, cache_spec],
        out_specs=(cache_spec, cache_spec),
    )(lengths, accepted, plane, cache_keys, cache_values)
    gates_out = kernel(gates_kernel, jax.ShapeDtypeStruct(cache_gates.shape, F32))(
        here(offsets), here(last), here(climb), gates
    )

    share = kernel(mix_kernel, near_memory((32, 128), F32))(here(everyone), here(w_out.T))
    shares = lax.all_gather(share, "tp")
    mixed = kernel(finish_kernel, jax.ShapeDtypeStruct((4, 32 // pair_count, 24), F32))(here(shares))
    mixed = jnp.swapaxes(mixed, 1, 2)
    return (mixed, keys_out, values_out, gates_out)


def solution(mesh):
    torus = Mesh(
        mesh.devices.reshape(mesh.shape["dp"], 16, 4, mesh.shape["tp"]),
        ("dp", "kv_0", "kv_1", "tp"),
    )
    return jax.shard_map(
        step,
        mesh=torus,
        in_specs=(
            P("dp", None, None),
            P(),
            P(KV, "tp"),
            P(KV, "tp"),
            P(KV, "tp"),
            P(KV, "tp"),
            P("tp"),
            P("tp"),
            P("tp", KV),
            P("dp", KV, "tp"),
            P("dp", KV, "tp"),
            P("dp", "tp", KV),
            P("dp"),
            P("dp"),
            P("dp", None),
        ),
        out_specs=(P("dp", None, KV_TP), P("dp", KV, "tp"), P("dp", KV, "tp"), P("dp", "tp", KV)),
        check_vma=False,
    )
```

time: 122 us -> 116 us (0.951)
  blocking collectives: 33.8 us -> 52.6 us
  waiting for transfers between devices: 34.2 us -> 20.5 us
  starting transfers between devices: 29.8 us -> 24 us
  Pallas kernels: 19.4 us -> 14.6 us
    all_to_all x3 -> x2, waiting for transfers between devices: 34.2 us -> 20.5 us  [spread(): return lax.all_to_all(array, axis, split_axis=0, concat_axis=0, tiled=True)]
    all_to_all x3, blocking collectives: 33.8 us -> 45.4 us  [spread(): return lax.all_to_all(array, axis, split_axis=0, concat_axis=0, tiled=True)]
    all_gather x0 -> x1, blocking collectives: none -> 7.18 us  [step(): shares = lax.all_gather(share, 'tp')]
    all_to_all x3 -> x2, starting transfers between devices: 29.8 us -> 24 us  [spread(): return lax.all_to_all(array, axis, split_axis=0, concat_axis=0, tiled=True)]
    pallas_call x8 -> x6, Pallas kernels: 13.3 us -> 8.51 us  [the longest x1 4.21 us: step(): kernel(attend_kernel, (near_memory((16, 4, 8, 128), BF16), near_memory((3...]
  transfers between devices with their start and end apart: 3 -> 2, of which waited for: 3 -> 2; matrix products, arithmetic and copies ran while one was open for 2% -> 2% of each run, Pallas kernels for 7% -> 6%
where the time goes in v3:
time: 116 us
  blocking collectives  52.6 us (45%)
  starting transfers between devices  24 us (21%)
  waiting for transfers between devices  20.5 us (18%)
  Pallas kernels  14.6 us (13%)
  local copies, waits for them, and re-layouts  3.03 us (3%)
    all_to_all x3, blocking collectives, spread(): return lax.all_to_all(array, axis, split_axis=0, concat_axis=0, tiled=True)  45.4 us
    all_to_all x2, starting transfers between devices, spread(): return lax.all_to_all(array, axis, split_axis=0, concat_axis=0, tiled=True)  24 us
    all_to_all x2, waiting for transfers between devices, spread(): return lax.all_to_all(array, axis, split_axis=0, concat_axis=0, tiled=True)  20.5 us
    all_gather x1, blocking collectives, step(): shares = lax.all_gather(share, 'tp')  7.18 us
    pallas_call x1, Pallas kernels, step(): kernel(attend_kernel, (near_memory((16, 4, 8, 128), BF16), near_memory((3...  4.21 us
    pallas_call x1, Pallas kernels, step(): kernel(write_kernel, (jax.ShapeDtypeStruct(cache_keys.shape, BF16), jax.S...  3.82 us
  transfers between devices with their start and end apart: 2, of which 2 were waited for; matrix products, arithmetic and copies ran while one was open for 2% of the time, Pallas kernels for 6%

profile of v3, /device:TPU:1, one launch (start us, length us, event | category | flops | bytes accessed | tf_op | source)
XLA Modules:
  0.0 115.6 jit_solution(381123251928592504)
XLA Ops:
  0.6 1.6 %shard_map.175 = bf16[64,8,128]{2,1,0:T(8,128)(2,1)} custom-call(bf16[32,512]{1,0:T(8,128)(2,1)} %wq_ref.1, bf16[32,512]{1,0:T(8,128)(2,1)} %wk_ref.1, bf16[32,512]{1,0:T(8,128)(2,1)} %wv_ref.1, bf16[8,32]{1,0:T(8,128)(2,1)} %bitcast.11), custom_call_target="tpu_custom_call" | custom-call | tf_op jit(solution)/shard_map/pallas_call | solution.py:329
  2.2 19.4 %all-to-all-start = ((bf16[64,8,128]{2,1,0:T(8,128)(2,1)}), bf16[64,8,128]{2,1,0:T(8,128)(2,1)S(1)}, u32[]{:S(2)}, u32[]{:S(2)}) async-start(bf16[64,8,128]{2,1,0:T(8,128)(2,1)} %shard_map.175), calls=%async_computation | async-start | bytes 262144 | tf_op jit(solution)/shard_map/all_to_all | solution.py:293
  21.6 0.0 copy-start.4
  21.7 0.6 reshape.39.gain_ref
  22.3 0.1 copy-done.4
  22.3 0.1 lt.19
  22.4 0.1 div.10
  22.5 0.1 rem.19
  22.6 0.1 ne.25
  22.7 0.1 fusion.3
  22.8 0.6 reshape.40.par_ref
  23.4 0.7 copy-done.6
  24.1 0.7 copy.19.bias_ref
  24.7 1.9 %shard_map.174 = (bf16[128,2048]{1,0:T(8,128)(2,1)S(1)}, f32[128,128]{1,0:T(8,128)S(1)}, f32[128,128]{1,0:T(8,128)S(1)}, s32[8,128]{1,0:T(8,128)S(1)}, f32[8,128...) custom-call(s32[4]{0:T(128)} %len_ref.3, s32[4]{0:T(128)} %acc_ref.3, bf16[4,24,2048]{2,1,0:T(8,128)(2,1)} %tok_ref.1, ...), custom_call_target="tpu_custom_call" | custom-call | tf_op jit(solution)/shard_map/pallas_call | solution.py:341
  26.7 10.0 %all-to-all-done.x_ref = bf16[64,8,128]{2,1,0:T(8,128)(2,1)S(1)} async-done(((bf16[64,8,128]{2,1,0:T(8,128)(2,1)}), bf16[64,8,128]{2,1,0:T(8,128)(2,1)S(1)}, u32[]{:S(2)}, u32[]{:S(2)}) %all-to-all-start) | async-done | bytes 131104 | tf_op jit(solution)/shard_map/all_to_all | solution.py:293
  36.7 0.3 shard_map.176
  37.0 0.0 copy-start
  37.0 16.2 %all_to_all.25 = bf16[16,3,8,128]{3,2,1,0:T(8,128)(2,1)S(1)} all-to-all(bf16[16,3,8,128]{3,2,1,0:T(8,128)(2,1)S(1)} %get-tuple-element.24), channel_id=1, replica_groups=mesh['dp'=4,'kv_0'=16,'kv_1'=4,'tp'=2] {'kv_0'}, dimensions={0} | all-to-all | bytes 196608 | tf_op jit(solution)/shard_map/all_to_all | solution.py:293
  53.3 0.1 broadcast_in_dim.12
  53.3 8.6 %all_to_all.26.g_ref = bf16[4,16,3,8,128]{4,3,2,1,0:T(8,128)(2,1)S(1)} all-to-all(bf16[4,16,3,8,128]{4,3,2,1,0:T(8,128)(2,1)S(1)} %broadcast_in_dim.12), channel_id=1, replica_groups=mesh['dp'=4,'kv_0'=16,'kv_1'=4,'tp'=2] {'kv_1'}, dimensions={0} | all-to-all | bytes 786432 | tf_op jit(solution)/shard_map/all_to_all | solution.py:293
  61.9 0.0 copy-done
  61.9 4.2 %shard_map.177 = (bf16[16,4,8,128]{3,2,1,0:T(8,128)(2,1)S(1)}, f32[3,8,128]{2,1,0:T(8,128)S(1)}, f32[8,128]{1,0:T(8,128)S(1)}) custom-call(s32[8,128]{1,0:T(8,128)S(1)} %get-tuple-element.20.off_ref, f32[8,128]{1,0:T(8,128)S(1)} %get-tuple-element.21.last_ref, bf16[4,16,3,8,128]{4,3,2,1,0:T(8,128)(2,1)S(1)} %all_to_all.26.g_ref, ...), custom_call_target="tpu_custom_call" | custom-call | tf_op jit(solution)/shard_map/pallas_call | solution.py:372
  66.2 20.6 %all_to_all.27.r_ref = bf16[64,8,128]{2,1,0:T(8,128)(2,1)S(1)} all-to-all(bf16[64,8,128]{2,1,0:T(8,128)(2,1)S(1)} %bitcast.7), channel_id=1, replica_groups=mesh['dp'=4,'kv_0'=16,'kv_1'=4,'tp'=2] {'kv_0','kv_1'}, dimensions={0} | all-to-all | bytes 262144 | tf_op jit(solution)/shard_map/all_to_all | solution.py:293
  86.8 1.0 shard_map.178
  87.8 4.6 %all-to-all-start.4 = ((bf16[64,8,128]{2,1,0:T(8,128)(2,1)}), bf16[64,8,128]{2,1,0:T(8,128)(2,1)S(1)}, u32[]{:S(2)}, u32[]{:S(2)}) async-start(bf16[64,8,128]{2,1,0:T(8,128)(2,1)} %get-tuple-element.31), calls=%async_computation.4 | async-start | bytes 262144 | tf_op jit(solution)/shard_map/all_to_all | solution.py:293
  92.4 3.8 %shard_map.181 = (bf16[4,256,512]{2,1,0:T(8,128)(2,1)}, bf16[4,256,512]{2,1,0:T(8,128)(2,1)}) custom-call(s32[4]{0:T(128)} %len_ref.3, s32[4]{0:T(128)} %acc_ref.3, bf16[4,16,3,8,128]{4,3,2,1,0:T(8,128)(2,1)S(1)} %all_to_all.26.g_ref, bf16[4,256,512]{2,1,0:T(8,128)(2,1)} %k_ref.3, bf16[4,256,512]{2,1,0:T(8,128)(2,1)} %v_ref.3), custom_call_target="tpu_custom_call" | custom-call | tf_op jit(solution)/shard_map/pallas_call | solution.py:393
  96.2 0.9 shard_map.182
  97.1 10.5 %all-to-all-done.4.g_ref = bf16[64,8,128]{2,1,0:T(8,128)(2,1)S(1)} async-done(((bf16[64,8,128]{2,1,0:T(8,128)(2,1)}), bf16[64,8,128]{2,1,0:T(8,128)(2,1)S(1)}, u32[]{:S(2)}, u32[]{:S(2)}) %all-to-all-start.4) | async-done | bytes 131104 | tf_op jit(solution)/shard_map/all_to_all | solution.py:293
  107.5 0.0 copy-done.3
  107.6 0.2 shard_map.179
  107.7 7.2 %all-gather = f32[64,128]{1,0:T(8,128)S(1)} all-gather(f32[32,128]{1,0:T(8,128)S(1)} %shard_map.179), channel_id=2, replica_groups=mesh['dp'=4,'kv_0'=16,'kv_1'=4,'tp'=2] {'tp'}, dimensions={0}, use_global_device_ids=true | all-gather | bytes 49152 | tf_op jit(solution)/shard_map/all_gather | solution.py:408
  114.9 0.7 shard_map.180
  (12 shorter events, 0.0 us)
Async XLA Ops:
  2.2 19.4 %copy-start.5 = (bf16[2048]{0:T(1024)(128)(2,1)S(1)}, bf16[2048]{0:T(1024)(128)(2,1)}, u32[]{:S(2)}) copy-start(bf16[2048]{0:T(1024)(128)(2,1)} %param.16) | copy-start | bytes 12292
  2.2 34.5 %all-to-all-start = ((bf16[64,8,128]{2,1,0:T(8,128)(2,1)}), bf16[64,8,128]{2,1,0:T(8,128)(2,1)S(1)}, u32[]{:S(2)}, u32[]{:S(2)}) async-start(bf16[64,8,128]{2,1,0:T(8,128)(2,1)} %shard_map.175), calls=%async_computation | async-start | bytes 262144 | tf_op jit(solution)/shard_map/all_to_all | solution.py:293
  21.6 0.7 copy-start.4
  22.7 2.0 %copy-start.2 = (f32[4,8,256]{2,1,0:T(8,128)S(1)}, f32[4,8,256]{2,1,0:T(8,128)}, u32[]{:S(2)}) copy-start(f32[4,8,256]{2,1,0:T(8,128)} %gate_ref.5) | copy-start | bytes 98308
  23.4 0.7 copy-start.6
  36.7 25.2 %copy-start.1 = (bf16[4,256,512]{2,1,0:T(8,128)(2,1)S(1)}, bf16[4,256,512]{2,1,0:T(8,128)(2,1)}, u32[]{:S(2)}) copy-start(bf16[4,256,512]{2,1,0:T(8,128)(2,1)} %v_ref.3) | copy-start | bytes 3145732
  37.0 24.9 %copy-start = (bf16[4,256,512]{2,1,0:T(8,128)(2,1)S(1)}, bf16[4,256,512]{2,1,0:T(8,128)(2,1)}, u32[]{:S(2)}) copy-start(bf16[4,256,512]{2,1,0:T(8,128)(2,1)} %k_ref.3) | copy-start | bytes 3145732
  87.8 19.8 %all-to-all-start.4 = ((bf16[64,8,128]{2,1,0:T(8,128)(2,1)}), bf16[64,8,128]{2,1,0:T(8,128)(2,1)S(1)}, u32[]{:S(2)}, u32[]{:S(2)}) async-start(bf16[64,8,128]{2,1,0:T(8,128)(2,1)} %get-tuple-element.31), calls=%async_computation.4 | async-start | bytes 262144 | tf_op jit(solution)/shard_map/all_to_all | solution.py:293
  96.2 11.3 %copy-start.3 = (bf16[512,32]{0,1:T(8,128)(2,1)S(1)}, bf16[512,32]{0,1:T(8,128)(2,1)}, u32[]{:S(2)}) copy-start(bf16[512,32]{0,1:T(8,128)(2,1)} %param.23) | copy-start | bytes 98308

commit v4 on v3

--- a/solution.py
+++ b/solution.py
@@ -130,42 +130,47 @@
     out_ref, near_ref, climb_ref, q_ref,
 ):
     rows = k_ref.shape[1]
-    q_ref[...] = columns_of(g_ref, 0, 0, 16).T
+    q_ref[...] = columns_of(g_ref, 0, 0, 16).T * 0.125
+    half = iota((32, 128), 1) < 64
     lane = iota((64, 128), 1)
-    half = lane < 64
-    part = (lane % 64) // 8
     row = iota((64, 128), 0)
     mine = (lane % 8 == row % 8) & ((lane // 64) == (row // 32))
+    part = (iota((4, 8, 128), 2) % 64) // 8
     slot = iota((4, 8, 128), 1)
     last = last_ref[...][None]
-    for b in range(4):
-        gates = gate_ref[b]
-        seen = iota((64, rows), 1) < off_ref[b : b + 1, 0:1]
+
+    def scores_of(b):
+        found = []
         for p in range(4):
             q = q_ref[b * 32 : (b + 1) * 32, p * 128 : (p + 1) * 128]
-            both = jnp.concatenate([jnp.where(half[:32], q, 0.0), jnp.where(half[:32], 0.0, q)], axis=0).astype(BF16)
-            scores = lax.dot_general(
-                both, k_ref[b, :, p * 128 : (p + 1) * 128], NT, preferred_element_type=F32
-            ) * 0.125
-            shift = jnp.concatenate(
-                [jnp.broadcast_to(gates[2 * p + k : 2 * p + k + 1], (32, rows)) for k in range(2)], axis=0
+            both = jnp.concatenate([jnp.where(half, q, 0.0), jnp.where(half, 0.0, q)], axis=0).astype(BF16)
+            found.append(
+                lax.dot_general(both, k_ref[b, :, p * 128 : (p + 1) * 128], NT, preferred_element_type=F32)
             )
-            scores = jnp.where(seen, scores - shift, NEG_LARGE)
-            highest = jnp.max(scores, axis=1, keepdims=True)
-            weights = jnp.where(seen, jnp.exp(scores - highest), 0.0)
+        return found
+
+    ahead = scores_of(0)
+    for b in range(4):
+        scores, ahead = ahead, scores_of(b + 1) if b < 3 else None
+        off = off_ref[b : b + 1, 0:1]
+        gates = jnp.where(iota((8, rows), 1) < off, gate_ref[b], -NEG_LARGE)
+        for p in range(4):
+            shifts = [jnp.broadcast_to(gates[2 * p + k : 2 * p + k + 1], (32, rows)) for k in range(2)]
+            shifted = scores[p] - jnp.concatenate(shifts, axis=0)
+            highest = jnp.max(shifted, axis=1, keepdims=True)
+            weights = jnp.exp(shifted - highest)
             total = jnp.sum(weights, axis=1, keepdims=True)
             weighted = jnp.dot(
                 weights.astype(BF16), v_ref[b, :, p * 128 : (p + 1) * 128], preferred_element_type=F32
             )
-            some = total > 0.0
-            weighted = weighted * jnp.where(some, 1.0 / jnp.where(some, total, 1.0), 0.0)
-            level = jnp.where(some, highest + jnp.log(jnp.where(some, total, 1.0)), NEG_LARGE)
-            high, middle, low = three_parts(jnp.broadcast_to(level, (64, 128)))
-            value = jnp.where(part == 0, high, jnp.where(part == 1, middle, low))
-            value = jnp.where(mine & (part < 3), value, 0.0)
-            levels = jnp.sum((value[:32] + value[32:]).reshape(4, 8, 128), axis=1, keepdims=True)
-            pair = jnp.where(half[:32], weighted[:32], weighted[32:]).reshape(4, 8, 128)
-            pair = jnp.where(slot == 6, levels, jnp.where(slot == 7, last, pair))
+            weighted = weighted * (1.0 / total)
+            level = jnp.where(mine, highest + jnp.log(total), 0.0)
+            level = jnp.sum((level[:32] + level[32:]).reshape(4, 8, 128), axis=1, keepdims=True)
+            level = jnp.broadcast_to(jnp.where(off > 0, level, NEG_LARGE), (4, 8, 128))
+            high, middle, low = three_parts(level)
+            level = jnp.where(part == 0, high, jnp.where(part == 1, middle, low))
+            pair = jnp.where(half, weighted[:32], weighted[32:]).reshape(4, 8, 128)
+            pair = jnp.where(slot == 6, level, jnp.where(slot == 7, last, pair))
             out_ref[p * 4 : (p + 1) * 4, b] = pair.astype(BF16)
 
     parts = jnp.concatenate(three_parts(lg_ref[...]), axis=0).astype(BF16)
@@ -179,7 +184,7 @@
     values = columns_of(g_ref, 2, p * 4, 4).astype(BF16)
     q = q_ref[pl.ds(at, 8), pl.ds(pl.multiple_of(p * 128, 128), 128)]
     both = jnp.concatenate([jnp.where(half, q, 0.0), jnp.where(half, 0.0, q)], axis=0).astype(BF16)
-    near = jnp.dot(both, keys, preferred_element_type=F32) * 0.125
+    near = jnp.dot(both, keys, preferred_element_type=F32)
     head = iota((8, 128), 0)
     climbs = [jnp.sum(jnp.where(head == 2 * p + k, climb, 0.0), axis=0, keepdims=True) for k in range(2)]
     near = near - jnp.concatenate([jnp.broadcast_to(c, (8, 128)) for c in climbs], axis=0)

time: 116 us -> 113 us (0.974)
  Pallas kernels: 14.6 us -> 11.7 us
    pallas_call x1, Pallas kernels: 4.21 us -> 1.3 us  [step(): kernel(attend_kernel, (near_memory((16, 4, 8, 128), BF16), near_memory((3...]
where the time goes in v4:
time: 113 us
  blocking collectives  52.6 us (47%)
  starting transfers between devices  24 us (21%)
  waiting for transfers between devices  20.5 us (18%)
  Pallas kernels  11.7 us (10%)
  local copies, waits for them, and re-layouts  3.03 us (3%)
    all_to_all x3, blocking collectives, spread(): return lax.all_to_all(array, axis, split_axis=0, concat_axis=0, tiled=True)  45.4 us
    all_to_all x2, starting transfers between devices, spread(): return lax.all_to_all(array, axis, split_axis=0, concat_axis=0, tiled=True)  24 us
    all_to_all x2, waiting for transfers between devices, spread(): return lax.all_to_all(array, axis, split_axis=0, concat_axis=0, tiled=True)  20.5 us
    all_gather x1, blocking collectives, step(): shares = lax.all_gather(share, 'tp')  7.18 us
    pallas_call x1, Pallas kernels, step(): kernel(write_kernel, (jax.ShapeDtypeStruct(cache_keys.shape, BF16), jax.S...  3.82 us
  transfers between devices with their start and end apart: 2, of which 2 were waited for; matrix products, arithmetic and copies ran while one was open for 2% of the time, Pallas kernels for 6%

profile of v4, /device:TPU:1, one launch (start us, length us, event | category | flops | bytes accessed | tf_op | source)
XLA Modules:
  0.0 112.7 jit_solution(7411313193535590300)
XLA Ops:
  0.6 1.6 %shard_map.175 = bf16[64,8,128]{2,1,0:T(8,128)(2,1)} custom-call(bf16[32,512]{1,0:T(8,128)(2,1)} %wq_ref.1, bf16[32,512]{1,0:T(8,128)(2,1)} %wk_ref.1, bf16[32,512]{1,0:T(8,128)(2,1)} %wv_ref.1, bf16[8,32]{1,0:T(8,128)(2,1)} %bitcast.11), custom_call_target="tpu_custom_call" | custom-call | tf_op jit(solution)/shard_map/pallas_call | solution.py:334
  2.2 19.4 %all-to-all-start = ((bf16[64,8,128]{2,1,0:T(8,128)(2,1)}), bf16[64,8,128]{2,1,0:T(8,128)(2,1)S(1)}, u32[]{:S(2)}, u32[]{:S(2)}) async-start(bf16[64,8,128]{2,1,0:T(8,128)(2,1)} %shard_map.175), calls=%async_computation | async-start | bytes 262144 | tf_op jit(solution)/shard_map/all_to_all | solution.py:298
  21.6 0.0 copy-done.5
  21.6 0.0 copy-start.4
  21.7 0.6 reshape.39.gain_ref
  22.3 0.1 copy-done.4
  22.3 0.1 lt.19
  22.4 0.1 div.10
  22.5 0.1 rem.19
  22.6 0.1 ne.25
  22.7 0.1 fusion.3
  22.8 0.6 reshape.40.par_ref
  23.4 0.7 copy-done.6
  24.1 0.7 copy.19.bias_ref
  24.7 1.9 %shard_map.174 = (bf16[128,2048]{1,0:T(8,128)(2,1)S(1)}, f32[128,128]{1,0:T(8,128)S(1)}, f32[128,128]{1,0:T(8,128)S(1)}, s32[8,128]{1,0:T(8,128)S(1)}, f32[8,128...) custom-call(s32[4]{0:T(128)} %len_ref.3, s32[4]{0:T(128)} %acc_ref.3, bf16[4,24,2048]{2,1,0:T(8,128)(2,1)} %tok_ref.1, ...), custom_call_target="tpu_custom_call" | custom-call | tf_op jit(solution)/shard_map/pallas_call | solution.py:346
  26.7 10.0 %all-to-all-done.x_ref = bf16[64,8,128]{2,1,0:T(8,128)(2,1)S(1)} async-done(((bf16[64,8,128]{2,1,0:T(8,128)(2,1)}), bf16[64,8,128]{2,1,0:T(8,128)(2,1)S(1)}, u32[]{:S(2)}, u32[]{:S(2)}) %all-to-all-start) | async-done | bytes 131104 | tf_op jit(solution)/shard_map/all_to_all | solution.py:298
  36.7 0.3 shard_map.176
  37.0 0.0 copy-start
  37.0 16.2 %all_to_all.25 = bf16[16,3,8,128]{3,2,1,0:T(8,128)(2,1)S(1)} all-to-all(bf16[16,3,8,128]{3,2,1,0:T(8,128)(2,1)S(1)} %get-tuple-element.24), channel_id=1, replica_groups=mesh['dp'=4,'kv_0'=16,'kv_1'=4,'tp'=2] {'kv_0'}, dimensions={0} | all-to-all | bytes 196608 | tf_op jit(solution)/shard_map/all_to_all | solution.py:298
  53.3 0.1 broadcast_in_dim.12
  53.3 8.6 %all_to_all.26.g_ref = bf16[4,16,3,8,128]{4,3,2,1,0:T(8,128)(2,1)S(1)} all-to-all(bf16[4,16,3,8,128]{4,3,2,1,0:T(8,128)(2,1)S(1)} %broadcast_in_dim.12), channel_id=1, replica_groups=mesh['dp'=4,'kv_0'=16,'kv_1'=4,'tp'=2] {'kv_1'}, dimensions={0} | all-to-all | bytes 786432 | tf_op jit(solution)/shard_map/all_to_all | solution.py:298
  61.9 0.0 copy-done
  61.9 1.3 %shard_map.177 = (bf16[16,4,8,128]{3,2,1,0:T(8,128)(2,1)S(1)}, f32[3,8,128]{2,1,0:T(8,128)S(1)}, f32[8,128]{1,0:T(8,128)S(1)}) custom-call(s32[8,128]{1,0:T(8,128)S(1)} %get-tuple-element.20.off_ref, f32[8,128]{1,0:T(8,128)S(1)} %get-tuple-element.21.last_ref, bf16[4,16,3,8,128]{4,3,2,1,0:T(8,128)(2,1)S(1)} %all_to_all.26.g_ref, ...), custom_call_target="tpu_custom_call" | custom-call | tf_op jit(solution)/shard_map/pallas_call | solution.py:377
  63.3 20.6 %all_to_all.27.r_ref = bf16[64,8,128]{2,1,0:T(8,128)(2,1)S(1)} all-to-all(bf16[64,8,128]{2,1,0:T(8,128)(2,1)S(1)} %bitcast.7), channel_id=1, replica_groups=mesh['dp'=4,'kv_0'=16,'kv_1'=4,'tp'=2] {'kv_0','kv_1'}, dimensions={0} | all-to-all | bytes 262144 | tf_op jit(solution)/shard_map/all_to_all | solution.py:298
  83.8 1.0 shard_map.178
  84.9 4.6 %all-to-all-start.4 = ((bf16[64,8,128]{2,1,0:T(8,128)(2,1)}), bf16[64,8,128]{2,1,0:T(8,128)(2,1)S(1)}, u32[]{:S(2)}, u32[]{:S(2)}) async-start(bf16[64,8,128]{2,1,0:T(8,128)(2,1)} %get-tuple-element.31), calls=%async_computation.4 | async-start | bytes 262144 | tf_op jit(solution)/shard_map/all_to_all | solution.py:298
  89.5 3.8 %shard_map.181 = (bf16[4,256,512]{2,1,0:T(8,128)(2,1)}, bf16[4,256,512]{2,1,0:T(8,128)(2,1)}) custom-call(s32[4]{0:T(128)} %len_ref.3, s32[4]{0:T(128)} %acc_ref.3, bf16[4,16,3,8,128]{4,3,2,1,0:T(8,128)(2,1)S(1)} %all_to_all.26.g_ref, bf16[4,256,512]{2,1,0:T(8,128)(2,1)} %k_ref.3, bf16[4,256,512]{2,1,0:T(8,128)(2,1)} %v_ref.3), custom_call_target="tpu_custom_call" | custom-call | tf_op jit(solution)/shard_map/pallas_call | solution.py:398
  93.3 0.9 shard_map.182
  94.2 10.5 %all-to-all-done.4.g_ref = bf16[64,8,128]{2,1,0:T(8,128)(2,1)S(1)} async-done(((bf16[64,8,128]{2,1,0:T(8,128)(2,1)}), bf16[64,8,128]{2,1,0:T(8,128)(2,1)S(1)}, u32[]{:S(2)}, u32[]{:S(2)}) %all-to-all-start.4) | async-done | bytes 131104 | tf_op jit(solution)/shard_map/all_to_all | solution.py:298
  104.6 0.2 shard_map.179
  104.8 7.2 %all-gather = f32[64,128]{1,0:T(8,128)S(1)} all-gather(f32[32,128]{1,0:T(8,128)S(1)} %shard_map.179), channel_id=2, replica_groups=mesh['dp'=4,'kv_0'=16,'kv_1'=4,'tp'=2] {'tp'}, dimensions={0}, use_global_device_ids=true | all-gather | bytes 49152 | tf_op jit(solution)/shard_map/all_gather | solution.py:413
  112.0 0.7 shard_map.180
  (12 shorter events, 0.0 us)
Async XLA Ops:
  2.2 19.4 %copy-start.5 = (bf16[2048]{0:T(1024)(128)(2,1)S(1)}, bf16[2048]{0:T(1024)(128)(2,1)}, u32[]{:S(2)}) copy-start(bf16[2048]{0:T(1024)(128)(2,1)} %param.16) | copy-start | bytes 12292
  2.2 34.5 %all-to-all-start = ((bf16[64,8,128]{2,1,0:T(8,128)(2,1)}), bf16[64,8,128]{2,1,0:T(8,128)(2,1)S(1)}, u32[]{:S(2)}, u32[]{:S(2)}) async-start(bf16[64,8,128]{2,1,0:T(8,128)(2,1)} %shard_map.175), calls=%async_computation | async-start | bytes 262144 | tf_op jit(solution)/shard_map/all_to_all | solution.py:298
  21.6 0.7 copy-start.4
  22.7 2.0 %copy-start.2 = (f32[4,8,256]{2,1,0:T(8,128)S(1)}, f32[4,8,256]{2,1,0:T(8,128)}, u32[]{:S(2)}) copy-start(f32[4,8,256]{2,1,0:T(8,128)} %gate_ref.5) | copy-start | bytes 98308
  23.4 0.7 copy-start.6
  36.7 25.2 %copy-start.1 = (bf16[4,256,512]{2,1,0:T(8,128)(2,1)S(1)}, bf16[4,256,512]{2,1,0:T(8,128)(2,1)}, u32[]{:S(2)}) copy-start(bf16[4,256,512]{2,1,0:T(8,128)(2,1)} %v_ref.3) | copy-start | bytes 3145732
  37.0 24.9 %copy-start = (bf16[4,256,512]{2,1,0:T(8,128)(2,1)S(1)}, bf16[4,256,512]{2,1,0:T(8,128)(2,1)}, u32[]{:S(2)}) copy-start(bf16[4,256,512]{2,1,0:T(8,128)(2,1)} %k_ref.3) | copy-start | bytes 3145732
  84.9 19.8 %all-to-all-start.4 = ((bf16[64,8,128]{2,1,0:T(8,128)(2,1)}), bf16[64,8,128]{2,1,0:T(8,128)(2,1)S(1)}, u32[]{:S(2)}, u32[]{:S(2)}) async-start(bf16[64,8,128]{2,1,0:T(8,128)(2,1)} %get-tuple-element.31), calls=%async_computation.4 | async-start | bytes 262144 | tf_op jit(solution)/shard_map/all_to_all | solution.py:298
  93.3 11.3 %copy-start.3 = (bf16[512,32]{0,1:T(8,128)(2,1)S(1)}, bf16[512,32]{0,1:T(8,128)(2,1)}, u32[]{:S(2)}) copy-start(bf16[512,32]{0,1:T(8,128)(2,1)} %param.23) | copy-start | bytes 98308

commit v5 on v4

--- a/solution.py
+++ b/solution.py
@@ -42,10 +42,18 @@
         [wq_ref[...].astype(F32), wk_ref[...].astype(F32), wv_ref[...].astype(F32), jnp.zeros((rows, wq_ref.shape[1]), F32)],
         axis=0,
     )
-    turned = stacked.T.reshape(out_ref.shape)
+    turned = stacked.T
+    queries = turned.reshape(16, 4, 8, 128)
+    block = iota((128, 128), 1) // rows
+    line = queries[:, 0].reshape(128, 128)
+    for g in range(1, 4):
+        line = jnp.where(block == g, pltpu.roll(queries[:, g].reshape(128, 128), g * rows, 1), line)
+    line = jnp.broadcast_to(line.reshape(16, 1, 8, 128), (16, 4, 8, 128)).reshape(64, 8, 128)
+    out_ref[:, 0] = line.astype(BF16)
+    turned = turned.reshape(64, 8, 128)
     forget = jnp.concatenate([jnp.zeros((8, 3 * rows), F32), wf_ref[...].astype(F32)], axis=1)
     lane = iota((1, 8, 128), 2)
-    out_ref[...] = jnp.where(lane >= 3 * rows, forget[None], turned).astype(BF16)
+    out_ref[:, 1] = jnp.where(lane >= 3 * rows, forget[None], turned).astype(BF16)
 
 
 def prepare_kernel(
@@ -92,22 +100,23 @@
 
 
 def project_kernel(x_ref, nrm_ref, bias_ref, piece_ref, gate_ref, wt_ref):
-    x = x_ref[...].astype(F32).reshape(16, 4, 8, 128)
     block = iota((128, 128), 1) // 32
-    for t in range(4):
+    tiles = [x_ref[:, k].astype(F32).reshape(16, 4, 8, 128) for k in range(2)]
+    wanted = [(0, 0), (0, 1), (0, 2), (0, 3), (1, 1), (1, 2), (1, 3)]
+    for at, (k, t) in enumerate(wanted):
         row = None
         for n in range(4):
-            moved = x[:, n].reshape(128, 128)
+            moved = tiles[k][:, n].reshape(128, 128)
             if n != t:
                 moved = pltpu.roll(moved, ((n - t) * 32) % 128, 1)
             row = moved if row is None else jnp.where(block == n, moved, row)
         row = row.reshape(16, 8, 128)
         for m in range(16):
-            wt_ref[t * 8 : (t + 1) * 8, m * 128 : (m + 1) * 128] = row[m]
+            wt_ref[at * 8 : (at + 1) * 8, m * 128 : (m + 1) * 128] = row[m]
     out = lax.dot_general(wt_ref[...].astype(BF16), nrm_ref[...], NT, preferred_element_type=F32)
-    piece = out[:24].reshape(3, 8, 128).astype(BF16)
+    piece = out[:48].reshape(6, 8, 128).astype(BF16)
     piece_ref[...] = jnp.broadcast_to(piece[None], piece_ref.shape)
-    pre = out[24:] + bias_ref[...]
+    pre = out[48:] + bias_ref[...]
     gate_ref[...] = jnp.minimum(pre, 0.0) - jnp.log1p(jnp.exp(-jnp.abs(pre)))
 
 
@@ -125,12 +134,11 @@
     return jnp.stack(parts, axis=1).reshape(count * 32, 128)
 
 
-def attend_kernel(
-    off_ref, last_ref, g_ref, k_ref, v_ref, gate_ref, lg_ref, link_ref, turned_ref,
-    out_ref, near_ref, climb_ref, q_ref,
-):
+def attend_kernel(off_ref, last_ref, g_ref, k_ref, v_ref, gate_ref, out_ref, own_ref, query_ref, q_ref):
     rows = k_ref.shape[1]
-    q_ref[...] = columns_of(g_ref, 0, 0, 16).T * 0.125
+    own_ref[...] = g_ref[:, 4:]
+    q_ref[...] = g_ref[:, :4].astype(F32).reshape(512, 128).T * 0.125
+    query_ref[...] = q_ref[...]
     half = iota((32, 128), 1) < 64
     lane = iota((64, 128), 1)
     row = iota((64, 128), 0)
@@ -173,6 +181,8 @@
             pair = jnp.where(slot == 6, level, jnp.where(slot == 7, last, pair))
             out_ref[p * 4 : (p + 1) * 4, b] = pair.astype(BF16)
 
+
+def near_kernel(g_ref, q_ref, lg_ref, link_ref, turned_ref, near_ref, climb_ref):
     parts = jnp.concatenate(three_parts(lg_ref[...]), axis=0).astype(BF16)
     summed = jnp.dot(parts, link_ref[...].astype(BF16), preferred_element_type=F32)
     climb = summed[:8] + summed[8:16] + summed[16:]
@@ -180,8 +190,8 @@
     p, group, seq = merger(lax.axis_index(KV))
     half = iota((8, 128), 1) < 64
     at = pl.multiple_of(seq * 32 + group * 8, 8)
-    keys = columns_of(g_ref, 1, p * 4, 4).astype(BF16)
-    values = columns_of(g_ref, 2, p * 4, 4).astype(BF16)
+    keys = columns_of(g_ref, 0, p * 4, 4).astype(BF16)
+    values = columns_of(g_ref, 1, p * 4, 4).astype(BF16)
     q = q_ref[pl.ds(at, 8), pl.ds(pl.multiple_of(p * 128, 128), 128)]
     both = jnp.concatenate([jnp.where(half, q, 0.0), jnp.where(half, 0.0, q)], axis=0).astype(BF16)
     near = jnp.dot(both, keys, preferred_element_type=F32)
@@ -216,7 +226,7 @@
         placed = placement(b, off, rows).astype(F32).astype(BF16)
         index = iota((rows, 512), 0)
         landed = (index >= off) & (index < off + 24)
-        for n, source, target in ((1, k_ref, kout_ref), (2, v_ref, vout_ref)):
+        for n, source, target in ((0, k_ref, kout_ref), (1, v_ref, vout_ref)):
             fresh = columns_of(g_ref, n, 0, 16).astype(BF16)
             written = lax.dot_general(placed, fresh, NT, preferred_element_type=F32)
             target[0] = jnp.where(landed, written, source[0].astype(F32)).astype(BF16)
@@ -292,6 +302,9 @@
         for b in range(4):
             at = (g * 4 + b) * SLOTS
             out_ref[b, :, g * GROUP : (g + 1) * GROUP] = total[:, at : at + GROUP]
+
+
+GRANTS = {project_kernel: 16 * 2**20, attend_kernel: 16 * 2**20}
 
 
 def spread(array, axis):
@@ -329,9 +342,10 @@
     vmem = pl.BlockSpec(memory_space=pltpu.VMEM)
 
     def kernel(body, out_shape, **kw):
-        return pl.pallas_call(body, out_shape=out_shape, interpret=INTERPRET, **kw)
-
-    packed = kernel(pack_kernel, near_memory((64, 8, 128), BF16))(w_query, w_key, w_value, w_forget.T)
+        params = pltpu.CompilerParams(vmem_limit_bytes=GRANTS.get(body))
+        return pl.pallas_call(body, out_shape=out_shape, interpret=INTERPRET, compiler_params=params, **kw)
+
+    packed = kernel(pack_kernel, near_memory((64, 2, 8, 128), BF16))(w_query, w_key, w_value, w_forget.T)
     columns = spread(packed, KV)
 
     groups = parents.reshape(4, 4, GROUP)
@@ -368,28 +382,22 @@
     )
     pieces, log_gate = kernel(
         project_kernel,
-        (near_memory((16, 3, 8, 128), BF16), small),
-        scratch_shapes=[pltpu.VMEM((32, 2048), F32)],
+        (near_memory((16, 6, 8, 128), BF16), small),
+        scratch_shapes=[pltpu.VMEM((56, 2048), F32)],
     )(here(columns), here(normed), here(bias))
     line = spread(pieces, KV[0])
-    plane = here(spread(jnp.broadcast_to(line[None], (4, *line.shape)), KV[1]))
-
-    partial, near, climb = kernel(
+    partial, own, query = kernel(
         attend_kernel,
-        (near_memory((16, 4, 8, 128), BF16), near_memory((3, 8, 128), F32), small),
+        (near_memory((16, 4, 8, 128), BF16), near_memory((16, 2, 8, 128), BF16), near_memory((128, 512), F32)),
         scratch_shapes=[pltpu.VMEM((128, 512), F32)],
-    )(
-        here(offsets),
-        here(last_part),
-        plane,
-        keys,
-        values,
-        gates,
-        here(log_gate),
-        here(link),
-        here(turned),
-    )
+    )(here(offsets), here(last_part), here(line), keys, values, gates)
     received = spread(partial.reshape(64, 8, 128), KV)
+    two = lax.all_gather(own, KV[1], axis_index_groups=[[0, 1], [2, 3]])
+    plane = lax.all_gather(two, KV[1], axis_index_groups=[[0, 3], [1, 2]])
+    plane = here(plane.reshape(4, *own.shape))
+    near, climb = kernel(near_kernel, (near_memory((3, 8, 128), F32), small))(
+        plane, here(query), here(log_gate), here(link), here(turned)
+    )
     heads, last = kernel(merge_kernel, (near_memory((64, 8, 128), BF16), small))(
         here(received), here(near), here(own_gain)
     )

time: 113 us -> 120 us (1.062)
  blocking collectives: 52.6 us -> 34.6 us
  starting transfers between devices: 24 us -> 38.7 us
  waiting for transfers between devices: 20.5 us -> 30.1 us
    all_to_all x3 -> x1, blocking collectives: 45.4 us -> 17.3 us  [spread(): return lax.all_to_all(array, axis, split_axis=0, concat_axis=0, tiled=True)]
    all_to_all x2 -> x3, starting transfers between devices: 24 us -> 38.7 us  [spread(): return lax.all_to_all(array, axis, split_axis=0, concat_axis=0, tiled=True)]
    all_gather x0 -> x2, blocking collectives: none -> 10 us  [the longest x1 6.22 us: step(): plane = lax.all_gather(two, KV[1], axis_index_groups=[[0, 3], [1, 2]])]
    all_to_all x2 -> x3, waiting for transfers between devices: 20.5 us -> 30.1 us  [spread(): return lax.all_to_all(array, axis, split_axis=0, concat_axis=0, tiled=True)]
    pallas_call x3 -> x4, Pallas kernels: 3.21 us -> 4.19 us  [the longest x1 1.76 us: step(): kernel(attend_kernel, (near_memory((16, 4, 8, 128), BF16), near_memory((1...]
  transfers between devices with their start and end apart: 2 -> 3, of which waited for: 2 -> 3; matrix products, arithmetic and copies ran while one was open for 2% -> 2% of each run, Pallas kernels for 6% -> 6%
where the time goes in v5:
time: 120 us; the launch traced here: 119 us
  starting transfers between devices  38.7 us (32%)
  blocking collectives  34.6 us (29%)
  waiting for transfers between devices  30.1 us (25%)
  Pallas kernels  12.7 us (11%)
  local copies, waits for them, and re-layouts  2.26 us (2%)
    all_to_all x3, starting transfers between devices, spread(): return lax.all_to_all(array, axis, split_axis=0, concat_axis=0, tiled=True)  38.7 us
    all_to_all x3, waiting for transfers between devices, spread(): return lax.all_to_all(array, axis, split_axis=0, concat_axis=0, tiled=True)  30.1 us
    all_to_all x1, blocking collectives, spread(): return lax.all_to_all(array, axis, split_axis=0, concat_axis=0, tiled=True)  17.3 us
    all_gather x1, blocking collectives, step(): shares = lax.all_gather(share, 'tp')  7.34 us
    all_gather x1, blocking collectives, step(): plane = lax.all_gather(two, KV[1], axis_index_groups=[[0, 3], [1, 2]])  6.22 us
    pallas_call x1, Pallas kernels, step(): kernel(write_kernel, (jax.ShapeDtypeStruct(cache_keys.shape, BF16), jax.S...  3.82 us
    all_gather x1, blocking collectives, step(): two = lax.all_gather(own, KV[1], axis_index_groups=[[0, 1], [2, 3]])  3.8 us
  transfers between devices with their start and end apart: 3, of which 3 were waited for; matrix products, arithmetic and copies ran while one was open for 2% of the time, Pallas kernels for 6%

profile of v5, /device:TPU:1, one launch (start us, length us, event | category | flops | bytes accessed | tf_op | source)
XLA Modules:
  0.0 119.3 jit_solution(2609557643593850762)
XLA Ops:
  0.6 0.0 copy-start.5
  0.6 0.0 copy-start.4
  0.7 0.0 copy-start.6
  0.7 1.7 %shard_map.175 = bf16[64,2,8,128]{3,2,1,0:T(8,128)(2,1)} custom-call(bf16[32,512]{1,0:T(8,128)(2,1)} %wq_ref.1, bf16[32,512]{1,0:T(8,128)(2,1)} %wk_ref.1, bf16[32,512]{1,0:T(8,128)(2,1)} %wv_ref.1, bf16[8,32]{1,0:T(8,128)(2,1)} %bitcast.12), custom_call_target="tpu_custom_call" | custom-call | tf_op jit(solution)/shard_map/pallas_call | solution.py:348
  2.4 19.4 %all-to-all-start = ((bf16[64,2,8,128]{3,2,1,0:T(8,128)(2,1)}), bf16[64,2,8,128]{3,2,1,0:T(8,128)(2,1)S(1)}, u32[]{:S(2)}, u32[]{:S(2)}) async-start(bf16[64,2,8,128]{3,2,1,0:T(8,128)(2,1)} %shard_map.175), calls=%async_computation | async-start | bytes 524288 | tf_op jit(solution)/shard_map/all_to_all | solution.py:311
  21.8 0.6 reshape.41.gain_ref
  22.4 0.1 lt.19
  22.5 0.1 div.10
  22.6 0.1 rem.19
  22.7 0.1 ne.25
  22.8 0.1 fusion.3
  22.9 0.6 reshape.42.par_ref
  23.5 0.0 copy-done.6
  23.5 0.7 copy.20.bias_ref
  24.2 1.9 %shard_map.174 = (bf16[128,2048]{1,0:T(8,128)(2,1)S(1)}, f32[128,128]{1,0:T(8,128)S(1)}, f32[128,128]{1,0:T(8,128)S(1)}, s32[8,128]{1,0:T(8,128)S(1)}, f32[8,128...) custom-call(s32[4]{0:T(128)} %len_ref.3, s32[4]{0:T(128)} %acc_ref.3, bf16[4,24,2048]{2,1,0:T(8,128)(2,1)} %tok_ref.1, ...), custom_call_target="tpu_custom_call" | custom-call | tf_op jit(solution)/shard_map/pallas_call | solution.py:360
  26.1 15.2 %all-to-all-done.x_ref = bf16[64,2,8,128]{3,2,1,0:T(8,128)(2,1)S(1)} async-done(((bf16[64,2,8,128]{3,2,1,0:T(8,128)(2,1)}), bf16[64,2,8,128]{3,2,1,0:T(8,128)(2,1)S(1)}, u32[]{:S(2)}, u32[]{:S(2)}) %all-to-all-start) | async-done | bytes 262176 | tf_op jit(solution)/shard_map/all_to_all | solution.py:311
  41.3 0.4 shard_map.176
  41.7 17.3 %all_to_all.20.g_ref = bf16[16,6,8,128]{3,2,1,0:T(8,128)(2,1)S(1)} all-to-all(bf16[16,6,8,128]{3,2,1,0:T(8,128)(2,1)S(1)} %get-tuple-element.26), channel_id=1, replica_groups=mesh['dp'=4,'kv_0'=16,'kv_1'=4,'tp'=2] {'kv_0'}, dimensions={0} | all-to-all | bytes 393216 | tf_op jit(solution)/shard_map/all_to_all | solution.py:311
  58.9 1.8 %shard_map.177 = (bf16[16,4,8,128]{3,2,1,0:T(8,128)(2,1)}, bf16[16,2,8,128]{3,2,1,0:T(8,128)(2,1)S(1)}, f32[128,512]{1,0:T(8,128)S(1)}) custom-call(s32[8,128]{1,0:T(8,128)S(1)} %get-tuple-element.22.off_ref, f32[8,128]{1,0:T(8,128)S(1)} %get-tuple-element.23.last_ref, bf16[16,6,8,128]{3,2,1,0:T(8,128)(2,1)S(1)} %all_to_all.20.g_ref, ...), custom_call_target="tpu_custom_call" | custom-call | tf_op jit(solution)/shard_map/pallas_call | solution.py:389
  60.7 9.8 %all-to-all-start.2 = ((bf16[64,8,128]{2,1,0:T(8,128)(2,1)}), bf16[64,8,128]{2,1,0:T(8,128)(2,1)S(1)}, u32[]{:S(2)}, u32[]{:S(2)}) async-start(bf16[64,8,128]{2,1,0:T(8,128)(2,1)} %bitcast.3), calls=%async_computation.2 | async-start | bytes 262144 | tf_op jit(solution)/shard_map/all_to_all | solution.py:311
  70.5 3.8 %all-gather = bf16[32,2,8,128]{3,2,1,0:T(8,128)(2,1)S(1)} all-gather(bf16[16,2,8,128]{3,2,1,0:T(8,128)(2,1)S(1)} %get-tuple-element.28), channel_id=2, replica_groups={{0,2},{4,6},{1,3},{5,7},{8,10},{12,14},{9,11},{13,15},{16,18},{20,22},{..., dimensions={0}, use_global_device_ids=true | all-gather | bytes 196608 | tf_op jit(solution)/shard_map/all_gather | solution.py:395
  74.3 6.2 %all-gather.1.g_ref = bf16[4,16,2,8,128]{4,3,2,1,0:T(8,128)(2,1)S(1)} all-gather(bf16[2,16,2,8,128]{4,3,2,1,0:T(8,128)(2,1)S(1)} %bitcast.10), channel_id=3, replica_groups={{0,6},{2,4},{1,7},{3,5},{8,14},{10,12},{9,15},{11,13},{16,22},{18,20},{..., dimensions={0}, use_global_device_ids=true | all-gather | bytes 393216 | tf_op jit(solution)/shard_map/all_gather | solution.py:396
  80.5 0.3 shard_map.178
  80.8 4.6 %all-to-all-done.2.r_ref = bf16[64,8,128]{2,1,0:T(8,128)(2,1)S(1)} async-done(((bf16[64,8,128]{2,1,0:T(8,128)(2,1)}), bf16[64,8,128]{2,1,0:T(8,128)(2,1)S(1)}, u32[]{:S(2)}, u32[]{:S(2)}) %all-to-all-start.2) | async-done | bytes 131104 | tf_op jit(solution)/shard_map/all_to_all | solution.py:311
  85.5 1.0 shard_map.179
  86.5 9.5 %all-to-all-start.3 = ((bf16[64,8,128]{2,1,0:T(8,128)(2,1)}), bf16[64,8,128]{2,1,0:T(8,128)(2,1)S(1)}, u32[]{:S(2)}, u32[]{:S(2)}) async-start(bf16[64,8,128]{2,1,0:T(8,128)(2,1)} %get-tuple-element.35), calls=%async_computation.3 | async-start | bytes 262144 | tf_op jit(solution)/shard_map/all_to_all | solution.py:311
  96.1 3.8 %shard_map.182 = (bf16[4,256,512]{2,1,0:T(8,128)(2,1)}, bf16[4,256,512]{2,1,0:T(8,128)(2,1)}) custom-call(s32[4]{0:T(128)} %len_ref.3, s32[4]{0:T(128)} %acc_ref.3, bf16[4,16,2,8,128]{4,3,2,1,0:T(8,128)(2,1)S(1)} %all-gather.1.g_ref, bf16[4,256,512]{2,1,0:T(8,128)(2,1)} %k_ref.3, bf16[4,256,512]{2,1,0:T(8,128)(2,1)} %v_ref.3), custom_call_target="tpu_custom_call" | custom-call | tf_op jit(solution)/shard_map/pallas_call | solution.py:406
  99.9 0.9 shard_map.183
  100.7 10.3 %all-to-all-done.3.g_ref = bf16[64,8,128]{2,1,0:T(8,128)(2,1)S(1)} async-done(((bf16[64,8,128]{2,1,0:T(8,128)(2,1)}), bf16[64,8,128]{2,1,0:T(8,128)(2,1)S(1)}, u32[]{:S(2)}, u32[]{:S(2)}) %all-to-all-start.3) | async-done | bytes 131104 | tf_op jit(solution)/shard_map/all_to_all | solution.py:311
  111.0 0.2 shard_map.180
  111.2 7.3 %all-gather.2 = f32[64,128]{1,0:T(8,128)S(1)} all-gather(f32[32,128]{1,0:T(8,128)S(1)} %shard_map.180), channel_id=4, replica_groups=mesh['dp'=4,'kv_0'=16,'kv_1'=4,'tp'=2] {'tp'}, dimensions={0}, use_global_device_ids=true | all-gather | bytes 49152 | tf_op jit(solution)/shard_map/all_gather | solution.py:421
  118.6 0.7 shard_map.181
  (14 shorter events, 0.0 us)
Async XLA Ops:
  0.6 21.2 %copy-start.5 = (bf16[2048]{0:T(1024)(128)(2,1)S(1)}, bf16[2048]{0:T(1024)(128)(2,1)}, u32[]{:S(2)}) copy-start(bf16[2048]{0:T(1024)(128)(2,1)} %param.16) | copy-start | bytes 12292
  0.6 21.8 %copy-start.4 = (s32[4,24]{1,0:T(4,128)S(1)}, s32[4,24]{1,0:T(4,128)}, u32[]{:S(2)}) copy-start(s32[4,24]{1,0:T(4,128)} %param.29) | copy-start | bytes 1156
  0.7 22.8 %copy-start.6 = (f32[8]{0:T(128)S(1)}, f32[8]{0:T(128)}, u32[]{:S(2)}) copy-start(f32[8]{0:T(128)} %param.21) | copy-start | bytes 100
  0.7 23.5 %copy-start.2 = (f32[4,8,256]{2,1,0:T(8,128)S(1)}, f32[4,8,256]{2,1,0:T(8,128)}, u32[]{:S(2)}) copy-start(f32[4,8,256]{2,1,0:T(8,128)} %gate_ref.5) | copy-start | bytes 98308
  2.4 56.5 %copy-start = (bf16[4,256,512]{2,1,0:T(8,128)(2,1)S(1)}, bf16[4,256,512]{2,1,0:T(8,128)(2,1)}, u32[]{:S(2)}) copy-start(bf16[4,256,512]{2,1,0:T(8,128)(2,1)} %k_ref.3) | copy-start | bytes 3145732
  2.4 56.5 %copy-start.1 = (bf16[4,256,512]{2,1,0:T(8,128)(2,1)S(1)}, bf16[4,256,512]{2,1,0:T(8,128)(2,1)}, u32[]{:S(2)}) copy-start(bf16[4,256,512]{2,1,0:T(8,128)(2,1)} %v_ref.3) | copy-start | bytes 3145732
  2.4 38.9 %all-to-all-start = ((bf16[64,2,8,128]{3,2,1,0:T(8,128)(2,1)}), bf16[64,2,8,128]{3,2,1,0:T(8,128)(2,1)S(1)}, u32[]{:S(2)}, u32[]{:S(2)}) async-start(bf16[64,2,8,128]{3,2,1,0:T(8,128)(2,1)} %shard_map.175), calls=%async_computation | async-start | bytes 524288 | tf_op jit(solution)/shard_map/all_to_all | solution.py:311
  60.7 24.8 %all-to-all-start.2 = ((bf16[64,8,128]{2,1,0:T(8,128)(2,1)}), bf16[64,8,128]{2,1,0:T(8,128)(2,1)S(1)}, u32[]{:S(2)}, u32[]{:S(2)}) async-start(bf16[64,8,128]{2,1,0:T(8,128)(2,1)} %bitcast.3), calls=%async_computation.2 | async-start | bytes 262144 | tf_op jit(solution)/shard_map/all_to_all | solution.py:311
  86.5 24.5 %all-to-all-start.3 = ((bf16[64,8,128]{2,1,0:T(8,128)(2,1)}), bf16[64,8,128]{2,1,0:T(8,128)(2,1)S(1)}, u32[]{:S(2)}, u32[]{:S(2)}) async-start(bf16[64,8,128]{2,1,0:T(8,128)(2,1)} %get-tuple-element.35), calls=%async_computation.3 | async-start | bytes 262144 | tf_op jit(solution)/shard_map/all_to_all | solution.py:311
  99.9 11.2 %copy-start.3 = (bf16[512,32]{0,1:T(8,128)(2,1)S(1)}, bf16[512,32]{0,1:T(8,128)(2,1)}, u32[]{:S(2)}) copy-start(bf16[512,32]{0,1:T(8,128)(2,1)} %param.23) | copy-start | bytes 98308

commit v6 on v4

--- a/solution.py
+++ b/solution.py
@@ -7,8 +7,15 @@
 from jax.sharding import PartitionSpec as P
 
 
-KV = ("kv_0", "kv_1")
-KV_TP = ("kv_0", "kv_1", "tp")
+KV = "kv"
+KV_TP = ("kv", "tp")
+
+LINE, PLANE = 16, 4
+FIRST = (9, 2)
+MEMBERS = [(z + FIRST[0]) % LINE * PLANE + (y + FIRST[1]) % PLANE for z in range(LINE) for y in range(PLANE)]
+ALL = [MEMBERS]
+LINES = [MEMBERS[y::PLANE] for y in range(PLANE)]
+PLANES = [MEMBERS[z * PLANE : (z + 1) * PLANE] for z in range(LINE)]
 
 NEG_LARGE = -1e30
 EPSILON = 1e-06
@@ -33,7 +40,8 @@
 
 
 def merger(index):
-    return index // 16, (index // 4) % 4, index % 4
+    z = (index // PLANE + LINE - FIRST[0]) % LINE
+    return z // 4, z % 4, (index + PLANE - FIRST[1]) % PLANE
 
 
 def pack_kernel(wq_ref, wk_ref, wv_ref, wf_ref, out_ref):
@@ -63,7 +71,10 @@
         for g in range(4):
             at = b * 32 + g * SLOTS
             nrm_ref[at : at + GROUP, :] = normed[g * GROUP : (g + 1) * GROUP]
-    out_ref[...] = nrm_ref[...].astype(BF16)
+    for z in range(LINE):
+        at = (z + FIRST[0]) % LINE * 128
+        features = pltpu.roll(nrm_ref[:, at : at + 128], (PLANE - FIRST[1]) % PLANE * 32, 1)
+        out_ref[:, z * 128 : (z + 1) * 128] = features.astype(BF16)
 
     child = iota((128, 128), 0)
     linked = ((par_ref[...] == child) | (child == iota((128, 128), 1))).astype(F32)
@@ -294,8 +305,8 @@
             out_ref[b, :, g * GROUP : (g + 1) * GROUP] = total[:, at : at + GROUP]
 
 
-def spread(array, axis):
-    return lax.all_to_all(array, axis, split_axis=0, concat_axis=0, tiled=True)
+def spread(array, groups):
+    return lax.all_to_all(array, KV, split_axis=0, concat_axis=0, tiled=True, axis_index_groups=groups)
 
 
 def near_memory(shape, dtype):
@@ -332,7 +343,7 @@
         return pl.pallas_call(body, out_shape=out_shape, interpret=INTERPRET, **kw)
 
     packed = kernel(pack_kernel, near_memory((64, 8, 128), BF16))(w_query, w_key, w_value, w_forget.T)
-    columns = spread(packed, KV)
+    columns = spread(packed, ALL)
 
     groups = parents.reshape(4, 4, GROUP)
     groups = jnp.where(
@@ -371,8 +382,8 @@
         (near_memory((16, 3, 8, 128), BF16), small),
         scratch_shapes=[pltpu.VMEM((32, 2048), F32)],
     )(here(columns), here(normed), here(bias))
-    line = spread(pieces, KV[0])
-    plane = here(spread(jnp.broadcast_to(line[None], (4, *line.shape)), KV[1]))
+    line = spread(pieces, LINES)
+    plane = here(spread(jnp.broadcast_to(line[None], (4, *line.shape)), PLANES))
 
     partial, near, climb = kernel(
         attend_kernel,
@@ -389,11 +400,11 @@
         here(link),
         here(turned),
     )
-    received = spread(partial.reshape(64, 8, 128), KV)
+    received = spread(partial.reshape(64, 8, 128), ALL)
     heads, last = kernel(merge_kernel, (near_memory((64, 8, 128), BF16), small))(
         here(received), here(near), here(own_gain)
     )
-    everyone = spread(heads, KV)
+    everyone = spread(heads, ALL)
     cache_spec = pl.BlockSpec((1, rows, 512), lambda b: (b, 0, 0))
     keys_out, values_out = kernel(
         write_kernel,
@@ -418,8 +429,8 @@
 
 def solution(mesh):
     torus = Mesh(
-        mesh.devices.reshape(mesh.shape["dp"], 16, 4, mesh.shape["tp"]),
-        ("dp", "kv_0", "kv_1", "tp"),
+        mesh.devices.reshape(mesh.shape["dp"], LINE * PLANE, mesh.shape["tp"]),
+        ("dp", "kv", "tp"),
     )
     return jax.shard_map(
         step,

time: 113 us -> 106 us (0.938)
  waiting for transfers between devices: 20.5 us -> 2.48 us
  starting transfers between devices: 24 us -> 36.9 us
  blocking collectives: 52.6 us -> 50.5 us
    all_to_all x2, waiting for transfers between devices: 20.5 us -> 2.48 us  [spread(): lax.all_to_all(array, KV, split_axis=0, concat_axis=0, tiled=True, axis_i...]
    all_to_all x2, starting transfers between devices: 24 us -> 36.9 us  [spread(): lax.all_to_all(array, KV, split_axis=0, concat_axis=0, tiled=True, axis_i...]
    all_to_all x3, blocking collectives: 45.4 us -> 42.7 us  [spread(): lax.all_to_all(array, KV, split_axis=0, concat_axis=0, tiled=True, axis_i...]
where the time goes in v6:
time: 106 us; the launch traced here: 105 us
  blocking collectives  50.5 us (48%)
  starting transfers between devices  36.9 us (35%)
  Pallas kernels  11.7 us (11%)
  local copies, waits for them, and re-layouts  3.03 us (3%)
  waiting for transfers between devices  2.48 us (2%)
    all_to_all x3, blocking collectives, spread(): lax.all_to_all(array, KV, split_axis=0, concat_axis=0, tiled=True, axis_i...  42.7 us
    all_to_all x2, starting transfers between devices, spread(): lax.all_to_all(array, KV, split_axis=0, concat_axis=0, tiled=True, axis_i...  36.9 us
    all_gather x1, blocking collectives, step(): shares = lax.all_gather(share, 'tp')  7.85 us
    pallas_call x1, Pallas kernels, step(): kernel(write_kernel, (jax.ShapeDtypeStruct(cache_keys.shape, BF16), jax.S...  3.81 us
    all_to_all x2, waiting for transfers between devices, spread(): lax.all_to_all(array, KV, split_axis=0, concat_axis=0, tiled=True, axis_i...  2.48 us
  transfers between devices with their start and end apart: 2, of which 2 were waited for; matrix products, arithmetic and copies ran while one was open for 2% of the time, Pallas kernels for 6%

profile of v6, /device:TPU:1, one launch (start us, length us, event | category | flops | bytes accessed | tf_op | source)
XLA Modules:
  0.0 105.4 jit_solution(16140161427482201660)
XLA Ops:
  0.6 1.6 %shard_map.175 = bf16[64,8,128]{2,1,0:T(8,128)(2,1)} custom-call(bf16[32,512]{1,0:T(8,128)(2,1)} %wq_ref.1, bf16[32,512]{1,0:T(8,128)(2,1)} %wk_ref.1, bf16[32,512]{1,0:T(8,128)(2,1)} %wv_ref.1, bf16[8,32]{1,0:T(8,128)(2,1)} %bitcast.11), custom_call_target="tpu_custom_call" | custom-call | tf_op jit(solution)/shard_map/pallas_call | solution.py:345
  2.2 22.3 %all-to-all-start = ((bf16[64,8,128]{2,1,0:T(8,128)(2,1)}), bf16[64,8,128]{2,1,0:T(8,128)(2,1)S(1)}, u32[]{:S(2)}, u32[]{:S(2)}) async-start(bf16[64,8,128]{2,1,0:T(8,128)(2,1)} %shard_map.175), calls=%async_computation | async-start | bytes 262144 | tf_op jit(solution)/shard_map/all_to_all | solution.py:309
  24.6 0.0 copy-done.5
  24.6 0.0 copy-start.4
  24.6 0.6 reshape.39.gain_ref
  25.2 0.1 copy-done.4
  25.3 0.1 lt.19
  25.4 0.1 div.10
  25.4 0.1 rem.19
  25.5 0.1 ne.25
  25.6 0.1 fusion.3
  25.7 0.6 reshape.40.par_ref
  26.3 0.7 copy-done.6
  27.0 0.7 copy.19.bias_ref
  27.6 1.9 %shard_map.174 = (bf16[128,2048]{1,0:T(8,128)(2,1)S(1)}, f32[128,128]{1,0:T(8,128)S(1)}, f32[128,128]{1,0:T(8,128)S(1)}, s32[8,128]{1,0:T(8,128)S(1)}, f32[8,128...) custom-call(s32[4]{0:T(128)} %len_ref.3, s32[4]{0:T(128)} %acc_ref.3, bf16[4,24,2048]{2,1,0:T(8,128)(2,1)} %tok_ref.1, ...), custom_call_target="tpu_custom_call" | custom-call | tf_op jit(solution)/shard_map/pallas_call | solution.py:357
  29.5 2.1 %all-to-all-done.x_ref = bf16[64,8,128]{2,1,0:T(8,128)(2,1)S(1)} async-done(((bf16[64,8,128]{2,1,0:T(8,128)(2,1)}), bf16[64,8,128]{2,1,0:T(8,128)(2,1)S(1)}, u32[]{:S(2)}, u32[]{:S(2)}) %all-to-all-start) | async-done | bytes 131104 | tf_op jit(solution)/shard_map/all_to_all | solution.py:309
  31.6 0.3 shard_map.176
  31.9 0.0 copy-start
  31.9 15.5 %all_to_all.25 = bf16[16,3,8,128]{3,2,1,0:T(8,128)(2,1)S(1)} all-to-all(bf16[16,3,8,128]{3,2,1,0:T(8,128)(2,1)S(1)} %get-tuple-element.24), channel_id=1, replica_groups={{76,84,92,100,108,116,124,4,12,20,28,36,44,52,60,68},{78,86,94,102,110,..., dimensions={0} | all-to-all | bytes 196608 | tf_op jit(solution)/shard_map/all_to_all | solution.py:309
  47.5 0.1 broadcast_in_dim.12
  47.5 8.3 %all_to_all.26.g_ref = bf16[4,16,3,8,128]{4,3,2,1,0:T(8,128)(2,1)S(1)} all-to-all(bf16[4,16,3,8,128]{4,3,2,1,0:T(8,128)(2,1)S(1)} %broadcast_in_dim.12), channel_id=1, replica_groups={{76,78,72,74},{84,86,80,82},{92,94,88,90},{100,102,96,98},{108,110,104,..., dimensions={0} | all-to-all | bytes 786432 | tf_op jit(solution)/shard_map/all_to_all | solution.py:309
  55.8 1.3 %shard_map.177 = (bf16[16,4,8,128]{3,2,1,0:T(8,128)(2,1)S(1)}, f32[3,8,128]{2,1,0:T(8,128)S(1)}, f32[8,128]{1,0:T(8,128)S(1)}) custom-call(s32[8,128]{1,0:T(8,128)S(1)} %get-tuple-element.20.off_ref, f32[8,128]{1,0:T(8,128)S(1)} %get-tuple-element.21.last_ref, bf16[4,16,3,8,128]{4,3,2,1,0:T(8,128)(2,1)S(1)} %all_to_all.26.g_ref, ...), custom_call_target="tpu_custom_call" | custom-call | tf_op jit(solution)/shard_map/pallas_call | solution.py:388
  57.1 18.8 %all_to_all.27.r_ref = bf16[64,8,128]{2,1,0:T(8,128)(2,1)S(1)} all-to-all(bf16[64,8,128]{2,1,0:T(8,128)(2,1)S(1)} %bitcast.7), channel_id=1, replica_groups={{76,78,72,74,84,86,80,82,92,94,88,90,100,102,96,98,108,110,104,106,116,..., dimensions={0} | all-to-all | bytes 262144 | tf_op jit(solution)/shard_map/all_to_all | solution.py:309
  76.0 1.0 shard_map.178
  77.0 14.5 %all-to-all-start.4 = ((bf16[64,8,128]{2,1,0:T(8,128)(2,1)}), bf16[64,8,128]{2,1,0:T(8,128)(2,1)S(1)}, u32[]{:S(2)}, u32[]{:S(2)}) async-start(bf16[64,8,128]{2,1,0:T(8,128)(2,1)} %get-tuple-element.31), calls=%async_computation.4 | async-start | bytes 262144 | tf_op jit(solution)/shard_map/all_to_all | solution.py:309
  91.5 3.8 %shard_map.181 = (bf16[4,256,512]{2,1,0:T(8,128)(2,1)}, bf16[4,256,512]{2,1,0:T(8,128)(2,1)}) custom-call(s32[4]{0:T(128)} %len_ref.3, s32[4]{0:T(128)} %acc_ref.3, bf16[4,16,3,8,128]{4,3,2,1,0:T(8,128)(2,1)S(1)} %all_to_all.26.g_ref, bf16[4,256,512]{2,1,0:T(8,128)(2,1)} %k_ref.3, bf16[4,256,512]{2,1,0:T(8,128)(2,1)} %v_ref.3), custom_call_target="tpu_custom_call" | custom-call | tf_op jit(solution)/shard_map/pallas_call | solution.py:409
  95.4 0.9 shard_map.182
  96.2 0.4 all-to-all-done.4.g_ref
  96.6 0.0 copy-done.3
  96.6 0.2 shard_map.179
  96.8 7.9 %all-gather = f32[64,128]{1,0:T(8,128)S(1)} all-gather(f32[32,128]{1,0:T(8,128)S(1)} %shard_map.179), channel_id=2, replica_groups=mesh['dp'=4,'kv'=64,'tp'=2] {'tp'}, dimensions={0}, use_global_device_ids=true | all-gather | bytes 49152 | tf_op jit(solution)/shard_map/all_gather | solution.py:424
  104.6 0.7 shard_map.180
  (12 shorter events, 0.0 us)
Async XLA Ops:
  2.2 22.3 %copy-start.5 = (bf16[2048]{0:T(1024)(128)(2,1)S(1)}, bf16[2048]{0:T(1024)(128)(2,1)}, u32[]{:S(2)}) copy-start(bf16[2048]{0:T(1024)(128)(2,1)} %param.16) | copy-start | bytes 12292
  2.2 29.4 %all-to-all-start = ((bf16[64,8,128]{2,1,0:T(8,128)(2,1)}), bf16[64,8,128]{2,1,0:T(8,128)(2,1)S(1)}, u32[]{:S(2)}, u32[]{:S(2)}) async-start(bf16[64,8,128]{2,1,0:T(8,128)(2,1)} %shard_map.175), calls=%async_computation | async-start | bytes 262144 | tf_op jit(solution)/shard_map/all_to_all | solution.py:309
  24.6 0.7 copy-start.4
  25.6 2.0 %copy-start.2 = (f32[4,8,256]{2,1,0:T(8,128)S(1)}, f32[4,8,256]{2,1,0:T(8,128)}, u32[]{:S(2)}) copy-start(f32[4,8,256]{2,1,0:T(8,128)} %gate_ref.5) | copy-start | bytes 98308
  26.3 0.7 copy-start.6
  31.6 24.2 %copy-start.1 = (bf16[4,256,512]{2,1,0:T(8,128)(2,1)S(1)}, bf16[4,256,512]{2,1,0:T(8,128)(2,1)}, u32[]{:S(2)}) copy-start(bf16[4,256,512]{2,1,0:T(8,128)(2,1)} %v_ref.3) | copy-start | bytes 3145732
  31.9 23.9 %copy-start = (bf16[4,256,512]{2,1,0:T(8,128)(2,1)S(1)}, bf16[4,256,512]{2,1,0:T(8,128)(2,1)}, u32[]{:S(2)}) copy-start(bf16[4,256,512]{2,1,0:T(8,128)(2,1)} %k_ref.3) | copy-start | bytes 3145732
  77.0 19.6 %all-to-all-start.4 = ((bf16[64,8,128]{2,1,0:T(8,128)(2,1)}), bf16[64,8,128]{2,1,0:T(8,128)(2,1)S(1)}, u32[]{:S(2)}, u32[]{:S(2)}) async-start(bf16[64,8,128]{2,1,0:T(8,128)(2,1)} %get-tuple-element.31), calls=%async_computation.4 | async-start | bytes 262144 | tf_op jit(solution)/shard_map/all_to_all | solution.py:309
  95.4 1.3 %copy-start.3 = (bf16[512,32]{0,1:T(8,128)(2,1)S(1)}, bf16[512,32]{0,1:T(8,128)(2,1)}, u32[]{:S(2)}) copy-start(bf16[512,32]{0,1:T(8,128)(2,1)} %param.23) | copy-start | bytes 98308

commit v7 on v6

--- a/solution.py
+++ b/solution.py
@@ -11,7 +11,7 @@
 KV_TP = ("kv", "tp")
 
 LINE, PLANE = 16, 4
-FIRST = (9, 2)
+FIRST = (11, 2)
 MEMBERS = [(z + FIRST[0]) % LINE * PLANE + (y + FIRST[1]) % PLANE for z in range(LINE) for y in range(PLANE)]
 ALL = [MEMBERS]
 LINES = [MEMBERS[y::PLANE] for y in range(PLANE)]
@@ -219,8 +219,8 @@
 
     @pl.when(jnp.logical_not(landing))
     def _():
-        kout_ref[...] = k_ref[...]
-        vout_ref[...] = v_ref[...]
+        kout_ref[0] = k_ref[b]
+        vout_ref[0] = v_ref[b]
 
     @pl.when(landing)
     def _():
@@ -230,7 +230,7 @@
         for n, source, target in ((1, k_ref, kout_ref), (2, v_ref, vout_ref)):
             fresh = columns_of(g_ref, n, 0, 16).astype(BF16)
             written = lax.dot_general(placed, fresh, NT, preferred_element_type=F32)
-            target[0] = jnp.where(landed, written, source[0].astype(F32)).astype(BF16)
+            target[0] = jnp.where(landed, written, source[b].astype(F32)).astype(BF16)
 
 
 def merge_kernel(r_ref, near_ref, gain_ref, out_ref, last_ref):
@@ -266,8 +266,9 @@
     low = jnp.sum(jnp.where(half, square, 0.0), axis=1, keepdims=True)
     high = jnp.sum(jnp.where(half, 0.0, square), axis=1, keepdims=True)
     mean = jnp.where(half, low, high) * (1.0 / 64.0)
-    heads = (attended * lax.rsqrt(mean + EPSILON) * gain_ref[...]).astype(BF16)
-    out_ref[...] = jnp.broadcast_to(heads[None], out_ref.shape)
+    heads = attended * lax.rsqrt(mean + EPSILON) * gain_ref[...]
+    for k in range(3):
+        out_ref[:, k] = jnp.broadcast_to(heads[None, 2 * k : 2 * k + 2], (64, 2, 128)).astype(BF16)
 
 
 def gates_kernel(off_ref, last_ref, climb_ref, gate_ref, gout_ref):
@@ -285,10 +286,15 @@
         gout_ref[b] = jnp.where((spot >= off) & (spot < off + 24), written, gate_ref[b])
 
 
-def mix_kernel(g_ref, w_ref, out_ref):
+def mix_kernel(g_ref, w_ref, out_ref, slots_ref):
+    slots_ref[...] = jnp.zeros(slots_ref.shape, F32)
+    for i in range(64):
+        for k in range(3):
+            at = i * SLOTS + 2 * k
+            slots_ref[at : at + 2, :] = g_ref[i, k].astype(F32)
     total = jnp.zeros((32, 128), F32)
     for p in range(4):
-        heads = g_ref[p * 16 : (p + 1) * 16].astype(F32).reshape(128, 128).astype(BF16)
+        heads = slots_ref[p * 128 : (p + 1) * 128, :].astype(BF16)
         total = total + lax.dot_general(w_ref[:, p * 128 : (p + 1) * 128], heads, NT, preferred_element_type=F32)
     out_ref[...] = total.reshape(out_ref.shape)
 
@@ -303,6 +309,9 @@
         for b in range(4):
             at = (g * 4 + b) * SLOTS
             out_ref[b, :, g * GROUP : (g + 1) * GROUP] = total[:, at : at + GROUP]
+
+
+GRANTS = {body: 16 * 2**20 for body in (project_kernel, attend_kernel, merge_kernel, gates_kernel, write_kernel)}
 
 
 def spread(array, groups):
@@ -340,7 +349,8 @@
     vmem = pl.BlockSpec(memory_space=pltpu.VMEM)
 
     def kernel(body, out_shape, **kw):
-        return pl.pallas_call(body, out_shape=out_shape, interpret=INTERPRET, **kw)
+        params = pltpu.CompilerParams(vmem_limit_bytes=GRANTS.get(body))
+        return pl.pallas_call(body, out_shape=out_shape, interpret=INTERPRET, compiler_params=params, **kw)
 
     packed = kernel(pack_kernel, near_memory((64, 8, 128), BF16))(w_query, w_key, w_value, w_forget.T)
     columns = spread(packed, ALL)
@@ -401,7 +411,7 @@
         here(turned),
     )
     received = spread(partial.reshape(64, 8, 128), ALL)
-    heads, last = kernel(merge_kernel, (near_memory((64, 8, 128), BF16), small))(
+    heads, last = kernel(merge_kernel, (near_memory((64, 3, 2, 128), BF16), small))(
         here(received), here(near), here(own_gain)
     )
     everyone = spread(heads, ALL)
@@ -413,14 +423,16 @@
             jax.ShapeDtypeStruct(cache_values.shape, BF16),
         ),
         grid=(4,),
-        in_specs=[smem, smem, vmem, cache_spec, cache_spec],
+        in_specs=[smem, smem, vmem, vmem, vmem],
         out_specs=(cache_spec, cache_spec),
-    )(lengths, accepted, plane, cache_keys, cache_values)
+    )(lengths, accepted, plane, keys, values)
     gates_out = kernel(gates_kernel, jax.ShapeDtypeStruct(cache_gates.shape, F32))(
         here(offsets), here(last), here(climb), gates
     )
 
-    share = kernel(mix_kernel, near_memory((32, 128), F32))(here(everyone), here(w_out.T))
+    share = kernel(mix_kernel, near_memory((32, 128), F32), scratch_shapes=[pltpu.VMEM((512, 128), F32)])(
+        here(everyone), here(w_out.T)
+    )
     shares = lax.all_gather(share, "tp")
     mixed = kernel(finish_kernel, jax.ShapeDtypeStruct((4, 32 // pair_count, 24), F32))(here(shares))
     mixed = jnp.swapaxes(mixed, 1, 2)

time: 106 us -> 105 us (level)
  starting transfers between devices: 36.9 us -> 33.4 us
  waiting for transfers between devices: 2.48 us -> 5.66 us
  Pallas kernels: 11.7 us -> 10.4 us
  blocking collectives: 50.5 us -> 51.7 us
    all_to_all x2, starting transfers between devices: 36.9 us -> 33.4 us  [spread(): lax.all_to_all(array, KV, split_axis=0, concat_axis=0, tiled=True, axis_i...]
    all_to_all x2, waiting for transfers between devices: 2.48 us -> 5.66 us  [spread(): lax.all_to_all(array, KV, split_axis=0, concat_axis=0, tiled=True, axis_i...]
    all_to_all x3, blocking collectives: 42.7 us -> 45.3 us  [spread(): lax.all_to_all(array, KV, split_axis=0, concat_axis=0, tiled=True, axis_i...]
    all_gather x1, blocking collectives: 7.85 us -> 6.36 us  [step(): shares = lax.all_gather(share, 'tp')]
    pallas_call x1, Pallas kernels: 3.81 us -> 2.44 us  [step(): kernel(write_kernel, (jax.ShapeDtypeStruct(cache_keys.shape, BF16), jax.S...]
  transfers between devices with their start and end apart: 2 -> 2, of which waited for: 2 -> 2; matrix products, arithmetic and copies ran while one was open for 2% -> 2% of each run, Pallas kernels for 6% -> 5%
where the time goes in v7:
time: 105 us
  blocking collectives  51.7 us (49%)
  starting transfers between devices  33.4 us (32%)
  Pallas kernels  10.4 us (10%)
  waiting for transfers between devices  5.66 us (5%)
  local copies, waits for them, and re-layouts  3.04 us (3%)
    all_to_all x3, blocking collectives, spread(): lax.all_to_all(array, KV, split_axis=0, concat_axis=0, tiled=True, axis_i...  45.3 us
    all_to_all x2, starting transfers between devices, spread(): lax.all_to_all(array, KV, split_axis=0, concat_axis=0, tiled=True, axis_i...  33.4 us
    all_gather x1, blocking collectives, step(): shares = lax.all_gather(share, 'tp')  6.36 us
    all_to_all x2, waiting for transfers between devices, spread(): lax.all_to_all(array, KV, split_axis=0, concat_axis=0, tiled=True, axis_i...  5.66 us
    pallas_call x1, Pallas kernels, step(): kernel(write_kernel, (jax.ShapeDtypeStruct(cache_keys.shape, BF16), jax.S...  2.44 us
  transfers between devices with their start and end apart: 2, of which 2 were waited for; matrix products, arithmetic and copies ran while one was open for 2% of the time, Pallas kernels for 5%

profile of v7, /device:TPU:1, one launch (start us, length us, event | category | flops | bytes accessed | tf_op | source)
XLA Modules:
  0.0 104.9 jit_solution(721569453131674822)
XLA Ops:
  0.6 1.6 %shard_map.175 = bf16[64,8,128]{2,1,0:T(8,128)(2,1)} custom-call(bf16[32,512]{1,0:T(8,128)(2,1)} %wq_ref.1, bf16[32,512]{1,0:T(8,128)(2,1)} %wk_ref.1, bf16[32,512]{1,0:T(8,128)(2,1)} %wv_ref.1, bf16[8,32]{1,0:T(8,128)(2,1)} %bitcast.11), custom_call_target="tpu_custom_call" | custom-call | tf_op jit(solution)/shard_map/pallas_call | solution.py:355
  2.2 20.5 %all-to-all-start = ((bf16[64,8,128]{2,1,0:T(8,128)(2,1)}), bf16[64,8,128]{2,1,0:T(8,128)(2,1)S(1)}, u32[]{:S(2)}, u32[]{:S(2)}) async-start(bf16[64,8,128]{2,1,0:T(8,128)(2,1)} %shard_map.175), calls=%async_computation | async-start | bytes 262144 | tf_op jit(solution)/shard_map/all_to_all | solution.py:318
  22.7 0.0 copy-done.7
  22.7 0.0 copy-start.6
  22.7 0.6 reshape.39.gain_ref
  23.3 0.1 copy-done.6
  23.4 0.1 lt.19
  23.5 0.1 div.10
  23.6 0.1 rem.19
  23.7 0.1 ne.25
  23.8 0.1 fusion.3
  23.8 0.6 reshape.40.par_ref
  24.5 0.7 copy-done.8
  25.1 0.7 copy.19.bias_ref
  25.8 1.9 %shard_map.174 = (bf16[128,2048]{1,0:T(8,128)(2,1)S(1)}, f32[128,128]{1,0:T(8,128)S(1)}, f32[128,128]{1,0:T(8,128)S(1)}, s32[8,128]{1,0:T(8,128)S(1)}, f32[8,128...) custom-call(s32[4]{0:T(128)} %len_ref.3, s32[4]{0:T(128)} %acc_ref.3, bf16[4,24,2048]{2,1,0:T(8,128)(2,1)} %tok_ref.1, ...), custom_call_target="tpu_custom_call" | custom-call | tf_op jit(solution)/shard_map/pallas_call | solution.py:367
  27.7 2.8 %all-to-all-done.x_ref = bf16[64,8,128]{2,1,0:T(8,128)(2,1)S(1)} async-done(((bf16[64,8,128]{2,1,0:T(8,128)(2,1)}), bf16[64,8,128]{2,1,0:T(8,128)(2,1)S(1)}, u32[]{:S(2)}, u32[]{:S(2)}) %all-to-all-start) | async-done | bytes 131104 | tf_op jit(solution)/shard_map/all_to_all | solution.py:318
  30.5 0.3 shard_map.176
  30.8 16.6 %all_to_all.25 = bf16[16,3,8,128]{3,2,1,0:T(8,128)(2,1)S(1)} all-to-all(bf16[16,3,8,128]{3,2,1,0:T(8,128)(2,1)S(1)} %get-tuple-element.24), channel_id=1, replica_groups={{92,100,108,116,124,4,12,20,28,36,44,52,60,68,76,84},{94,102,110,118,12..., dimensions={0} | all-to-all | bytes 196608 | tf_op jit(solution)/shard_map/all_to_all | solution.py:318
  47.4 0.1 broadcast_in_dim.12
  47.5 8.9 %all_to_all.26.g_ref = bf16[4,16,3,8,128]{4,3,2,1,0:T(8,128)(2,1)S(1)} all-to-all(bf16[4,16,3,8,128]{4,3,2,1,0:T(8,128)(2,1)S(1)} %broadcast_in_dim.12), channel_id=1, replica_groups={{92,94,88,90},{100,102,96,98},{108,110,104,106},{116,118,112,114},{124,..., dimensions={0} | all-to-all | bytes 786432 | tf_op jit(solution)/shard_map/all_to_all | solution.py:318
  56.4 0.0 copy-done
  56.4 1.3 %shard_map.177 = (bf16[16,4,8,128]{3,2,1,0:T(8,128)(2,1)S(1)}, f32[3,8,128]{2,1,0:T(8,128)S(1)}, f32[8,128]{1,0:T(8,128)S(1)}) custom-call(s32[8,128]{1,0:T(8,128)S(1)} %get-tuple-element.20.off_ref, f32[8,128]{1,0:T(8,128)S(1)} %get-tuple-element.21.last_ref, bf16[4,16,3,8,128]{4,3,2,1,0:T(8,128)(2,1)S(1)} %all_to_all.26.g_ref, ...), custom_call_target="tpu_custom_call" | custom-call | tf_op jit(solution)/shard_map/pallas_call | solution.py:398
  57.7 19.7 %all_to_all.27.r_ref = bf16[64,8,128]{2,1,0:T(8,128)(2,1)S(1)} all-to-all(bf16[64,8,128]{2,1,0:T(8,128)(2,1)S(1)} %bitcast.7), channel_id=1, replica_groups={{92,94,88,90,100,102,96,98,108,110,104,106,116,118,112,114,124,126,120,..., dimensions={0} | all-to-all | bytes 262144 | tf_op jit(solution)/shard_map/all_to_all | solution.py:318
  77.4 1.1 %shard_map.178 = (bf16[64,3,2,128]{3,2,1,0:T(2,128)(2,1)}, f32[8,128]{1,0:T(8,128)S(1)}) custom-call(bf16[64,8,128]{2,1,0:T(8,128)(2,1)S(1)} %all_to_all.27.r_ref, f32[3,8,128]{2,1,0:T(8,128)S(1)} %get-tuple-element.29.near_ref, f32[8,128]{1,0:T(8,128)S(1)} %get-tuple-element.30.gain_ref), custom_call_target="tpu_custom_call" | custom-call | tf_op jit(solution)/shard_map/pallas_call | solution.py:414
  78.5 12.9 %all-to-all-start.4 = ((bf16[64,3,2,128]{3,2,1,0:T(2,128)(2,1)}), bf16[64,3,2,128]{3,2,1,0:T(2,128)(2,1)S(1)}, u32[]{:S(2)}, u32[]{:S(2)}) async-start(bf16[64,3,2,128]{3,2,1,0:T(2,128)(2,1)} %get-tuple-element.31), calls=%async_computation.4 | async-start | bytes 196608 | tf_op jit(solution)/shard_map/all_to_all | solution.py:318
  91.4 2.4 %shard_map.181 = (bf16[4,256,512]{2,1,0:T(8,128)(2,1)}, bf16[4,256,512]{2,1,0:T(8,128)(2,1)}) custom-call(s32[4]{0:T(128)S(1)} %copy-done.4, s32[4]{0:T(128)S(1)} %copy-done.5, bf16[4,16,3,8,128]{4,3,2,1,0:T(8,128)(2,1)S(1)} %all_to_all.26.g_ref, bf16[4,256,512]{2,1,0:T(8,128)(2,1)S(1)} %copy-done, bf16[4,256,512]{2,1,0:T(8,128)(2,1)S(1)} %copy-done.1), custom_call_target="tpu_custom_call" | custom-call | tf_op jit(solution)/shard_map/pallas_call | solution.py:419
  93.9 0.9 shard_map.182
  94.7 2.9 %all-to-all-done.4.g_ref = bf16[64,3,2,128]{3,2,1,0:T(2,128)(2,1)S(1)} async-done(((bf16[64,3,2,128]{3,2,1,0:T(2,128)(2,1)}), bf16[64,3,2,128]{3,2,1,0:T(2,128)(2,1)S(1)}, u32[]{:S(2)}, u32[]{:S(2)}) %all-to-all-start.4) | async-done | bytes 98336 | tf_op jit(solution)/shard_map/all_to_all | solution.py:318
  97.6 0.0 copy-done.3
  97.6 0.2 shard_map.179
  97.8 6.4 %all-gather = f32[64,128]{1,0:T(8,128)S(1)} all-gather(f32[32,128]{1,0:T(8,128)S(1)} %shard_map.179), channel_id=2, replica_groups=mesh['dp'=4,'kv'=64,'tp'=2] {'tp'}, dimensions={0}, use_global_device_ids=true | all-gather | bytes 49152 | tf_op jit(solution)/shard_map/all_gather | solution.py:436
  104.2 0.7 shard_map.180
  (16 shorter events, 0.0 us)
Async XLA Ops:
  2.2 20.5 %copy-start.7 = (bf16[2048]{0:T(1024)(128)(2,1)S(1)}, bf16[2048]{0:T(1024)(128)(2,1)}, u32[]{:S(2)}) copy-start(bf16[2048]{0:T(1024)(128)(2,1)} %param.16) | copy-start | bytes 12292
  2.2 28.2 %all-to-all-start = ((bf16[64,8,128]{2,1,0:T(8,128)(2,1)}), bf16[64,8,128]{2,1,0:T(8,128)(2,1)S(1)}, u32[]{:S(2)}, u32[]{:S(2)}) async-start(bf16[64,8,128]{2,1,0:T(8,128)(2,1)} %shard_map.175), calls=%async_computation | async-start | bytes 262144 | tf_op jit(solution)/shard_map/all_to_all | solution.py:318
  22.7 0.7 copy-start.6
  23.8 2.0 %copy-start.2 = (f32[4,8,256]{2,1,0:T(8,128)S(1)}, f32[4,8,256]{2,1,0:T(8,128)}, u32[]{:S(2)}) copy-start(f32[4,8,256]{2,1,0:T(8,128)} %gate_ref.5) | copy-start | bytes 98308
  24.5 0.7 copy-start.8
  30.5 25.9 %copy-start = (bf16[4,256,512]{2,1,0:T(8,128)(2,1)S(1)}, bf16[4,256,512]{2,1,0:T(8,128)(2,1)}, u32[]{:S(2)}) copy-start(bf16[4,256,512]{2,1,0:T(8,128)(2,1)} %k_ref.3) | copy-start | bytes 3145732
  30.5 25.9 %copy-start.1 = (bf16[4,256,512]{2,1,0:T(8,128)(2,1)S(1)}, bf16[4,256,512]{2,1,0:T(8,128)(2,1)}, u32[]{:S(2)}) copy-start(bf16[4,256,512]{2,1,0:T(8,128)(2,1)} %v_ref.3) | copy-start | bytes 3145732
  78.5 12.9 %copy-start.4 = (s32[4]{0:T(128)S(1)}, s32[4]{0:T(128)}, u32[]{:S(2)}) copy-start(s32[4]{0:T(128)} %len_ref.3) | copy-start | bytes 52
  78.5 12.9 %copy-start.5 = (s32[4]{0:T(128)S(1)}, s32[4]{0:T(128)}, u32[]{:S(2)}) copy-start(s32[4]{0:T(128)} %acc_ref.3) | copy-start | bytes 52
  78.5 19.1 %all-to-all-start.4 = ((bf16[64,3,2,128]{3,2,1,0:T(2,128)(2,1)}), bf16[64,3,2,128]{3,2,1,0:T(2,128)(2,1)S(1)}, u32[]{:S(2)}, u32[]{:S(2)}) async-start(bf16[64,3,2,128]{3,2,1,0:T(2,128)(2,1)} %get-tuple-element.31), calls=%async_computation.4 | async-start | bytes 196608 | tf_op jit(solution)/shard_map/all_to_all | solution.py:318
  93.9 3.7 %copy-start.3 = (bf16[512,32]{0,1:T(8,128)(2,1)S(1)}, bf16[512,32]{0,1:T(8,128)(2,1)}, u32[]{:S(2)}) copy-start(bf16[512,32]{0,1:T(8,128)(2,1)} %param.23) | copy-start | bytes 98308
